TPU v7x, 128 devices: a whole 4x4x4 slice. The times are simulated.
128 devices in a mesh: ep: 64 (over z, y, x), tp: 2 (over core).
Axes of the slice: x: 4, y: 4, z: 4, core: 2. Of those that a mesh axis runs over, the one named last changes fastest.
Arguments:
- stream: bfloat16 [4096, 2048], P('ep', 'tp'), may hold values from -40 to 40
- conv_state: bfloat16 [4096, 3, 2048], P('ep', None, 'tp'), may hold values from -5 to 5
- recur_state: float32 [4096, 2048], P('ep', 'tp'), may hold values from -5 to 5
- mix_gain: float32 [2048], replicated, may hold values from 0.1 to 1.9
- branch_weight: bfloat16 [2048, 2048], P(None, 'tp'), may hold values from -0.125 to 0.125
- gate_weight: bfloat16 [2048, 2048], P(None, 'tp'), may hold values from -0.125 to 0.125
- conv_taps: float32 [4, 2048], P(None, 'tp'), may hold values from -3 to 3
- recur_map: bfloat16 [16, 128, 128], P('tp'), may hold values from -0.5 to 0.5
- input_map: bfloat16 [16, 128, 128], P('tp'), may hold values from -0.5 to 0.5
- decay_logit: float32 [2048], P('tp'), may hold values from -1 to 6
- out_weight: bfloat16 [2048, 2048], P(None, 'tp'), may hold values from -0.125 to 0.125
- moe_gain: float32 [2048], replicated, may hold values from 0.1 to 1.9
- route_ids: int32 [4096, 6], P('ep'), may hold values from 0 to 63, all different within a row; in each aligned block of 64 rows (0 to 63, 64 to 127, ...) at most 18 rows name the same one
- route_weights: float32 [4096, 6], P('ep'), may hold values from 0.2 to 1
- expert_gate: bfloat16 [64, 2048, 512], P('ep', None, 'tp'), may hold values from -0.125 to 0.125
- expert_up: bfloat16 [64, 2048, 512], P('ep', None, 'tp'), may hold values from -0.125 to 0.125
- expert_down: bfloat16 [64, 512, 2048], P('ep', None, 'tp'), may hold values from -0.25 to 0.25
- dense_gate: bfloat16 [2048, 512], P(None, 'tp'), may hold values from -0.125 to 0.125
- dense_up: bfloat16 [2048, 512], P(None, 'tp'), may hold values from -0.125 to 0.125
- dense_down: bfloat16 [512, 2048], P(None, 'tp'), may hold values from -0.25 to 0.25
- dense_scale: float32 [2048], P('tp'), may hold values from 0.1 to 1.9
Outputs:
- result: bfloat16 [4096, 2048], P('ep', 'tp')
- new_state: float32 [4096, 2048], P('ep', 'tp')
- new_conv: bfloat16 [4096, 3, 2048], P('ep', None, 'tp')
Inputs may be any that keep to these rules, and one draw needn't show every extreme that they name: `route_ids`: each row names 6 different experts; among the rows of one index of ep no expert is named by more than 18 rows, and in every draw some expert is named by exactly 18 rows of some index.
All inputs are finite; a program needn't handle non-finite values.
Results may differ from a plain program's by a relative error of at most 0.014.
Values may be sent and summed in bfloat16 or wider, within the bound.
A program may use at most 128 MiB of HBM per device.

v0:
```python
import jax
import jax.numpy as jnp
from jax import lax
from jax.sharding import PartitionSpec as P


def laid_out(tiles, dim):
    shape = list(tiles.shape[1:])
    shape[dim] *= tiles.shape[0]
    return jnp.moveaxis(tiles, 0, dim).reshape(shape)


def sent_to_all(shard, axis):
    length = lax.axis_size(axis)
    return lax.all_to_all(
        jnp.broadcast_to(shard[None], (length, *shard.shape)), axis, 0, 0, tiled=True
    )


def gathered_copies(shard, axis, dim):
    return laid_out(sent_to_all(shard, axis), dim)


def accumulate_with(weight, segment):
    return jnp.dot(segment, weight, preferred_element_type=jnp.float32)


def normalize(part_rows, gain_vec):
    whole_rows = gathered_copies(part_rows, "tp", 1).astype(jnp.float32)
    row_mean = jnp.mean(whole_rows, axis=1, keepdims=True)
    row_var = jnp.mean(whole_rows * whole_rows, axis=1, keepdims=True) - row_mean * row_mean
    return ((whole_rows - row_mean) * lax.rsqrt(row_var + 1e-05) * gain_vec).astype(jnp.bfloat16)


def per_device(
    stream,
    conv_state,
    recur_state,
    mix_gain,
    branch_weight,
    gate_weight,
    conv_taps,
    recur_map,
    input_map,
    decay_logit,
    out_weight,
    moe_gain,
    route_ids,
    route_weights,
    expert_gate,
    expert_up,
    expert_down,
    dense_gate,
    dense_up,
    dense_down,
    dense_scale,
):
    seq_count = stream.shape[0]
    out_width = stream.shape[1]
    normed = normalize(stream, mix_gain)
    branch_in = jnp.dot(normed, branch_weight, preferred_element_type=jnp.float32).astype(
        jnp.bfloat16
    )
    gate_pre = jnp.dot(normed, gate_weight, preferred_element_type=jnp.float32).astype(jnp.bfloat16)
    conv_sum = branch_in.astype(jnp.float32) * conv_taps[3]
    for offset in range(3):
        conv_sum = conv_sum + conv_state[:, offset].astype(jnp.float32) * conv_taps[offset]
    conv_out = conv_sum.astype(jnp.bfloat16)
    new_conv = jnp.concatenate([conv_state[:, 1:], branch_in[:, None]], axis=1)
    block_count = recur_map.shape[0]
    block_width = recur_map.shape[1]
    grouped = conv_out.reshape(seq_count, block_count, block_width)
    recur_gate = jax.nn.sigmoid(
        jnp.einsum("nbc,bcd->nbd", grouped, recur_map, preferred_element_type=jnp.float32)
    ).reshape(seq_count, -1)
    input_gate = jax.nn.sigmoid(
        jnp.einsum("nbc,bcd->nbd", grouped, input_map, preferred_element_type=jnp.float32)
    ).reshape(seq_count, -1)
    log_decay = -8.0 * recur_gate * jax.nn.softplus(-decay_logit)
    driven = jnp.sqrt(-jnp.expm1(2.0 * log_decay)) * (input_gate * conv_out.astype(jnp.float32))
    new_state = jnp.exp(log_decay) * recur_state + driven
    mixer_in = (jax.nn.gelu(gate_pre.astype(jnp.float32)) * new_state).astype(jnp.bfloat16)
    mixer_out = accumulate_with(
        out_weight, lax.all_gather(mixer_in, "tp", axis=1, tiled=True)
    ).astype(jnp.bfloat16)
    resid = (stream.astype(jnp.float32) + mixer_out.astype(jnp.float32)).astype(jnp.bfloat16)
    normed_two = normalize(resid, moe_gain)
    top_count = route_ids.shape[1]
    expert_count = lax.axis_size("ep")
    capacity = max(2, min(seq_count, 3 * seq_count * top_count // expert_count))
    flat_ids = route_ids.reshape(-1)
    one_hot = (flat_ids[:, None] == jnp.arange(expert_count, dtype=jnp.int32)[None, :]).astype(
        jnp.int32
    )
    slot_rank = jnp.sum(one_hot * (jnp.cumsum(one_hot, axis=0) - 1), axis=1)
    slot_index = (flat_ids * capacity + slot_rank).reshape(seq_count, top_count)
    dispatch_table = jnp.sum(
        (
            slot_index[:, :, None]
            == jnp.arange(expert_count * capacity, dtype=jnp.int32)[None, None, :]
        ).astype(jnp.bfloat16),
        axis=1,
    )
    own_gate = expert_gate[0]
    own_up = expert_up[0]
    own_down = expert_down[0]
    own_features = lax.dynamic_slice_in_dim(
        normed_two, lax.axis_index("tp") * out_width, out_width, 1
    )
    outgoing = lax.dot_general(
        dispatch_table, own_features, (((0,), (0,)), ((), ())), preferred_element_type=jnp.float32
    )
    outgoing = outgoing.astype(jnp.bfloat16).reshape(expert_count, capacity, -1)
    incoming = lax.all_gather(
        lax.all_to_all(outgoing, "ep", split_axis=0, concat_axis=0, tiled=True),
        "tp",
        axis=2,
        tiled=True,
    )
    source_count, slot_count, feature_count = incoming.shape
    taken_rows = incoming.reshape(source_count * slot_count, feature_count)
    gate_sum = jnp.dot(taken_rows, own_gate, preferred_element_type=jnp.float32)
    up_sum = jnp.dot(taken_rows, own_up, preferred_element_type=jnp.float32)
    hidden = (jax.nn.silu(gate_sum) * up_sum).astype(jnp.bfloat16)
    served_rows = accumulate_with(own_down, gathered_copies(hidden, "tp", 1))
    served = served_rows.astype(jnp.bfloat16).reshape(source_count, slot_count, -1)
    returned = lax.all_to_all(served, "ep", split_axis=0, concat_axis=0, tiled=True).reshape(
        expert_count * capacity, -1
    )
    picked = returned[slot_index]
    routed = jnp.sum(picked.astype(jnp.float32) * route_weights[:, :, None], axis=1)
    dense_gsum = jnp.dot(normed_two, dense_gate, preferred_element_type=jnp.float32)
    dense_usum = jnp.dot(normed_two, dense_up, preferred_element_type=jnp.float32)
    dense_hidden = (jax.nn.silu(dense_gsum) * dense_usum).astype(jnp.bfloat16)
    dense_out = accumulate_with(
        dense_down, lax.all_gather(dense_hidden, "tp", axis=1, tiled=True)
    ).astype(jnp.bfloat16)
    result = (
        resid.astype(jnp.float32) + routed + dense_scale * dense_out.astype(jnp.float32)
    ).astype(jnp.bfloat16)
    return (result, new_state, new_conv)


def solution(mesh):
    in_specs = (
        P("ep", "tp"),
        P("ep", None, "tp"),
        P("ep", "tp"),
        P(),
        P(None, "tp"),
        P(None, "tp"),
        P(None, "tp"),
        P("tp", None, None),
        P("tp", None, None),
        P("tp"),
        P(None, "tp"),
        P(),
        P("ep", None),
        P("ep", None),
        P("ep", None, "tp"),
        P("ep", None, "tp"),
        P("ep", None, "tp"),
        P(None, "tp"),
        P(None, "tp"),
        P(None, "tp"),
        P("tp"),
    )
    out_specs = (P("ep", "tp"), P("ep", "tp"), P("ep", None, "tp"))
    return jax.shard_map(
        per_device, mesh=mesh, in_specs=in_specs, out_specs=out_specs, check_vma=False
    )
```

profile of v0, /device:TPU:0, one launch (start us, length us, event | category | flops | bytes accessed | tf_op | source)
XLA Modules:
  0.0 197.2 jit_solution(7304002262852420736)
XLA Ops:
  7.2 0.0 copy-start
  7.2 0.0 copy-start.6
  7.2 1.7 broadcast_in_dim.10
  8.9 3.4 %all-to-all-start = ((bf16[2,64,1024]{2,1,0:T(8,128)(2,1)}), bf16[2,64,1024]{2,1,0:T(8,128)(2,1)S(1)}, u32[]{:S(2)}, u32[]{:S(2)}) async-start(bf16[2,64,1024]{2,1,0:T(8,128)(2,1)} %broadcast_in_dim.10), calls=%async_computation | async-start | bytes 524288 | tf_op jit(solution)/shard_map/all_to_all | solution.py:15
  12.4 0.9 fusion.51
  13.3 0.7 all-to-all-done
  14.0 0.2 convert_reduce_fusion.1
  14.2 0.0 copy-start.23
  14.3 0.0 copy-start.3
  14.3 4.0 %fusion.38 = (bf16[64,1024]{1,0:T(8,128)(2,1)S(1)}, bf16[64,1024]{1,0:T(8,128)(2,1)}) fusion(f32[1024]{0:T(1024)S(1)} %bitcast.101, bf16[64,3,1024]{2,0,1:T(8,128)(2,1)S(1)} %copy-done.6, f32[1024]{0:T(1024)S(1)} %bitcast.102, f32[1024]{0:T(1024)S(1)} %bitcast.100, f32[1024]{0:T(1024)S(1)} %bitcast.99, bf16[2048,1024]{1,0:T(8,128)(2,1)} %param.25, ...), kind=kOutput, calls=%fused_computation.64 | convolution fusion | flops 269811712 | bytes 5399040 | tf_op jit(solution)/shard_map/dot_general | solution.py:61
  18.2 0.2 fusion.5
  18.5 0.2 fusion.9
  18.7 0.2 copy-done.19
  18.9 0.3 copy-done.13
  19.2 0.2 fusion.36
  19.4 0.0 copy-start.9
  19.5 1.0 fusion.34
  20.5 2.1 %all_gather.9 = bf16[64,2048]{1,0:T(8,128)(2,1)S(1)} all-gather(bf16[64,1024]{1,0:T(8,128)(2,1)S(1)} %fusion.34), channel_id=1, replica_groups=mesh['ep'=64,'tp'=2] {'tp'}, dimensions={1}, use_global_device_ids=true | all-gather | bytes 393216 | tf_op jit(solution)/shard_map/all_gather | solution.py:84
  22.6 0.9 fusion.15
  23.5 0.7 broadcast_in_dim.11
  24.2 3.4 %all-to-all-start.1 = ((bf16[2,64,1024]{2,1,0:T(8,128)(2,1)}), bf16[2,64,1024]{2,1,0:T(8,128)(2,1)S(1)}, u32[]{:S(2)}, u32[]{:S(2)}) async-start(bf16[2,64,1024]{2,1,0:T(8,128)(2,1)} %broadcast_in_dim.11), calls=%async_computation.1 | async-start | bytes 524288 | tf_op jit(solution)/shard_map/all_to_all | solution.py:15
  27.6 0.0 all-gather.2.cloned.1.call-start
  27.7 0.1 copy.73
  27.8 0.1 eq.38
  27.9 0.1 eq.42
  28.1 1.1 all-to-all-done.1
  29.3 0.9 reduce-window.6
  30.2 0.2 slice_reduce_fusion
  30.5 0.1 fusion.47
  30.6 0.1 reduce_sum.71
  30.7 0.1 copy.76
  30.8 1.0 fusion.23
  31.8 0.2 convert_reduce_fusion
  32.0 0.1 multiply_convert_fusion
  32.2 0.7 copy-done.4
  32.9 1.7 convolution_convert_fusion.1
  34.6 2.4 %reshape.118 = bf16[64,18,1024]{2,1,0:T(8,128)(2,1)} reshape(bf16[1152,1024]{1,0:T(8,128)(2,1)S(1)} %convolution_convert_fusion.1) | data formatting | bytes 4718592 | tf_op jit(solution)/shard_map/reshape | solution.py:113
  37.0 53.3 %all_to_all.25 = bf16[64,18,1024]{2,1,0:T(8,128)(2,1)} all-to-all(bf16[64,18,1024]{2,1,0:T(8,128)(2,1)} %reshape.118), channel_id=1, replica_groups=mesh['ep'=64,'tp'=2] {'ep'}, dimensions={0} | all-to-all | bytes 4718592 | tf_op jit(solution)/shard_map/all_to_all | solution.py:115
  90.3 0.0 all-gather.2.cloned.1.call-update
  90.3 15.6 %all-gather.2.cloned.1.call-done = bf16[64,18,2048]{2,1,0:T(8,128)(2,1)} async-done(((bf16[64,18,1024]{2,1,0:T(8,128)(2,1)}), bf16[64,18,2048]{2,1,0:T(8,128)(2,1)}) %all-gather.2.cloned.1.call-update) | async-done | bytes 4718608 | tf_op jit(solution)/shard_map/all_gather | solution.py:114
  106.0 7.8 %reshape.119 = bf16[1152,2048]{1,0:T(8,128)(2,1)} reshape(bf16[64,18,2048]{2,1,0:T(8,128)(2,1)} %all-gather.2.cloned.1.call-done) | data formatting | bytes 9437184 | tf_op jit(solution)/shard_map/reshape | solution.py:121
  113.7 3.9 %fusion.21 = f32[1152,256]{1,0:T(8,128)S(1)} fusion(bf16[1152,2048]{1,0:T(8,128)(2,1)} %reshape.119, bf16[1,2048,256]{2,1,0:T(8,128)(2,1)S(1)} %copy-done.20), kind=kOutput, calls=%fused_computation.34 | convolution fusion | flops 1207959552 | bytes 6946816 | tf_op jit(solution)/shard_map/dot_general | solution.py:122
  117.7 0.1 copy-done.21
  117.8 1.6 fusion
  119.4 0.3 copy.78
  119.7 0.1 broadcast_in_dim.12
  119.8 4.7 %all_to_all.26 = bf16[2,1152,256]{1,2,0:T(8,128)(2,1)S(1)} all-to-all(bf16[2,1152,256]{1,2,0:T(8,128)(2,1)S(1)} %broadcast_in_dim.12), channel_id=1, replica_groups=mesh['ep'=64,'tp'=2] {'tp'}, dimensions={0} | all-to-all | bytes 2359296 | tf_op jit(solution)/shard_map/all_to_all | solution.py:15
  124.4 1.4 convolution_convert_fusion
  125.9 2.4 %reshape.121 = bf16[64,18,1024]{2,1,0:T(8,128)(2,1)} reshape(bf16[1152,1024]{1,0:T(8,128)(2,1)S(1)} %convolution_convert_fusion) | data formatting | bytes 4718592 | tf_op jit(solution)/shard_map/reshape | solution.py:126
  128.3 10.8 %all-to-all-start.4 = ((bf16[64,18,1024]{2,1,0:T(8,128)(2,1)}), bf16[64,18,1024]{2,1,0:T(8,128)(2,1)}, u32[]{:S(2)}, u32[]{:S(2)}) async-start(bf16[64,18,1024]{2,1,0:T(8,128)(2,1)} %reshape.121), calls=%async_computation.4 | async-start | bytes 6291456 | tf_op jit(solution)/shard_map/all_to_all | solution.py:127
  139.1 0.0 slice-start
  139.1 0.1 copy.79
  139.2 0.1 reshape.130
  139.3 0.7 copy.80
  140.1 0.3 fusion.52
  140.4 1.5 fusion.18
  141.9 2.0 %all_gather.11 = bf16[64,512]{1,0:T(8,128)(2,1)} all-gather(bf16[64,256]{1,0:T(8,128)(2,1)S(1)} %fusion.18), channel_id=1, replica_groups=mesh['ep'=64,'tp'=2] {'tp'}, dimensions={1}, use_global_device_ids=true | all-gather | bytes 98304 | tf_op jit(solution)/shard_map/all_gather | solution.py:136
  143.9 0.8 pad_maximum_fusion
  144.7 36.2 %all-to-all-done.4 = bf16[64,18,1024]{2,1,0:T(8,128)(2,1)} async-done(((bf16[64,18,1024]{2,1,0:T(8,128)(2,1)}), bf16[64,18,1024]{2,1,0:T(8,128)(2,1)}, u32[]{:S(2)}, u32[]{:S(2)}) %all-to-all-start.4) | async-done | bytes 2359328 | tf_op jit(solution)/shard_map/all_to_all | solution.py:127
  180.9 2.9 %reshape.122 = bf16[1152,1024]{1,0:T(8,128)(2,1)S(1)} reshape(bf16[64,18,1024]{2,1,0:T(8,128)(2,1)} %all-to-all-done.4) | data formatting | bytes 4718592 | tf_op jit(solution)/shard_map/reshape | solution.py:127
  183.8 2.7 %gather_fusion = bf16[384,1024]{1,0:T(8,128)(2,1)} fusion(bf16[1152,1024]{1,0:T(8,128)(2,1)S(1)} %reshape.122, s32[1024]{0:T(1024)S(1)} %pad_clamp_fusion), kind=kCustom, calls=%fused_computation | custom fusion | bytes 1574400 | tf_op jit(solution)/shard_map/gather | solution.py:130
  186.5 1.3 reshape.138
  187.8 1.6 multiply_reduce_fusion
  189.4 1.0 fusion.17
  (51 shorter events, 0.3 us)
Async XLA Ops:
  7.2 117.3 %copy-start = (bf16[1,512,1024]{2,1,0:T(8,128)(2,1)S(1)}, bf16[1,512,1024]{2,1,0:T(8,128)(2,1)}, u32[]{:S(2)}) copy-start(bf16[1,512,1024]{2,1,0:T(8,128)(2,1)} %param.37) | copy-start | bytes 3145732
  7.2 7.0 %copy-start.6 = (bf16[64,3,1024]{2,0,1:T(8,128)(2,1)S(1)}, bf16[64,3,1024]{2,0,1:T(8,128)(2,1)}, u32[]{:S(2)}) copy-start(bf16[64,3,1024]{2,0,1:T(8,128)(2,1)} %param.22) | copy-start | bytes 1179652
  7.2 7.0 %copy-start.14 = (f32[2048]{0:T(1024)S(1)}, f32[2048]{0:T(1024)}, u32[]{:S(2)}) copy-start(f32[2048]{0:T(1024)} %param.24) | copy-start | bytes 24580
  8.9 5.0 %all-to-all-start = ((bf16[2,64,1024]{2,1,0:T(8,128)(2,1)}), bf16[2,64,1024]{2,1,0:T(8,128)(2,1)S(1)}, u32[]{:S(2)}, u32[]{:S(2)}) async-start(bf16[2,64,1024]{2,1,0:T(8,128)(2,1)} %broadcast_in_dim.10), calls=%async_computation | async-start | bytes 524288 | tf_op jit(solution)/shard_map/all_to_all | solution.py:15
  14.2 4.0 %copy-start.22 = (bf16[8,128,128]{2,1,0:T(8,128)(2,1)S(1)}, bf16[8,128,128]{2,1,0:T(8,128)(2,1)}, u32[]{:S(2)}) copy-start(bf16[8,128,128]{2,1,0:T(8,128)(2,1)} %param.29) | copy-start | bytes 786436
  14.2 4.2 %copy-start.23 = (bf16[8,128,128]{2,1,0:T(8,128)(2,1)S(1)}, bf16[8,128,128]{2,1,0:T(8,128)(2,1)}, u32[]{:S(2)}) copy-start(bf16[8,128,128]{2,1,0:T(8,128)(2,1)} %param.28) | copy-start | bytes 786436
  14.3 5.2 %copy-start.3 = (bf16[2048,1024]{1,0:T(8,128)(2,1)S(1)}, bf16[2048,1024]{1,0:T(8,128)(2,1)}, u32[]{:S(2)}) copy-start(bf16[2048,1024]{1,0:T(8,128)(2,1)} %param.26) | copy-start | bytes 12582916
  18.2 0.7 copy-start.19
  18.2 1.0 copy-start.13
  19.4 1.0 copy-start.9
  19.4 3.1 %copy-start.2 = (bf16[2048,1024]{1,0:T(8,128)(2,1)S(1)}, bf16[2048,1024]{1,0:T(8,128)(2,1)}, u32[]{:S(2)}) copy-start(bf16[2048,1024]{1,0:T(8,128)(2,1)} %param.31) | copy-start | bytes 12582916
  19.5 3.1 %copy-start.10 = (bf16[64,1024]{1,0:T(8,128)(2,1)S(1)}, bf16[64,1024]{1,0:T(8,128)(2,1)}, u32[]{:S(2)}) copy-start(bf16[64,1024]{1,0:T(8,128)(2,1)} %param.21) | copy-start | bytes 393220
  22.6 5.1 %copy-start.15 = (s32[64,6]{0,1:T(8,128)S(1)}, s32[64,6]{0,1:T(8,128)}, u32[]{:S(2)}) copy-start(s32[64,6]{0,1:T(8,128)} %param.33) | copy-start | bytes 4612
  23.4 8.6 %copy-start.16 = (f32[2048]{0:T(1024)S(1)}, f32[2048]{0:T(1024)}, u32[]{:S(2)}) copy-start(f32[2048]{0:T(1024)} %param.32) | copy-start | bytes 24580
  24.2 5.0 %all-to-all-start.1 = ((bf16[2,64,1024]{2,1,0:T(8,128)(2,1)}), bf16[2,64,1024]{2,1,0:T(8,128)(2,1)S(1)}, u32[]{:S(2)}, u32[]{:S(2)}) async-start(bf16[2,64,1024]{2,1,0:T(8,128)(2,1)} %broadcast_in_dim.11), calls=%async_computation.1 | async-start | bytes 524288 | tf_op jit(solution)/shard_map/all_to_all | solution.py:15
  27.6 78.3 %all-gather.2.cloned.1.call-start = ((), (), s32[]{:S(2)}) async-start(), calls=%async_computation.5 | async-start | bytes 9437184 | tf_op jit(solution)/shard_map/all_gather | solution.py:114
  32.1 0.7 copy-start.4
  90.3 23.4 %copy-start.20 = (bf16[1,2048,256]{2,1,0:T(8,128)(2,1)S(1)}, bf16[1,2048,256]{2,1,0:T(8,128)(2,1)}, u32[]{:S(2)}) copy-start(bf16[1,2048,256]{2,1,0:T(8,128)(2,1)} %param.35) | copy-start | bytes 3145732
  113.7 3.9 %copy-start.1 = (bf16[1152,2048]{1,0:T(8,128)(2,1)S(1)}, bf16[1152,2048]{1,0:T(8,128)(2,1)}, u32[]{:S(2)}) copy-start(bf16[1152,2048]{1,0:T(8,128)(2,1)} %reshape.119) | copy-start | bytes 14155780
  113.7 4.1 %copy-start.21 = (bf16[1,2048,256]{2,1,0:T(8,128)(2,1)S(1)}, bf16[1,2048,256]{2,1,0:T(8,128)(2,1)}, u32[]{:S(2)}) copy-start(bf16[1,2048,256]{2,1,0:T(8,128)(2,1)} %param.36) | copy-start | bytes 3145732
  128.3 11.0 %copy-start.18 = (f32[64,6]{0,1:T(8,128)S(1)}, f32[64,6]{0,1:T(8,128)}, u32[]{:S(2)}) copy-start(f32[64,6]{0,1:T(8,128)} %param.34) | copy-start | bytes 4612
  128.3 11.7 %copy-start.5 = (bf16[64,2048]{1,0:T(8,128)(2,1)S(1)}, bf16[64,2048]{1,0:T(8,128)(2,1)}, u32[]{:S(2)}) copy-start(bf16[64,2048]{1,0:T(8,128)(2,1)} %copy-done.4) | copy-start | bytes 786436
  128.3 11.7 %copy-start.7 = (bf16[2048,256]{1,0:T(8,128)(2,1)S(1)}, bf16[2048,256]{1,0:T(8,128)(2,1)}, u32[]{:S(2)}) copy-start(bf16[2048,256]{1,0:T(8,128)(2,1)} %param.38) | copy-start | bytes 3145732
  128.3 52.5 %all-to-all-start.4 = ((bf16[64,18,1024]{2,1,0:T(8,128)(2,1)}), bf16[64,18,1024]{2,1,0:T(8,128)(2,1)}, u32[]{:S(2)}, u32[]{:S(2)}) async-start(bf16[64,18,1024]{2,1,0:T(8,128)(2,1)} %reshape.121), calls=%async_computation.4 | async-start | bytes 6291456 | tf_op jit(solution)/shard_map/all_to_all | solution.py:127
  139.1 4.8 %slice-start = ((bf16[64,3,1024]{2,0,1:T(8,128)(2,1)}), bf16[64,2,1024]{2,0,1:T(8,128)(2,1)S(1)}, s32[]{:S(2)}) async-start(bf16[64,3,1024]{2,0,1:T(8,128)(2,1)} %param.22), calls=%async_computation.6 | async-start | bytes 524288 | tf_op jit(solution)/shard_map/slice | solution.py:69
  139.1 4.8 %copy-start.11 = (bf16[64,1024]{1,0:T(8,128)(2,1)S(1)}, bf16[64,1024]{1,0:T(8,128)(2,1)}, u32[]{:S(2)}) copy-start(bf16[64,1024]{1,0:T(8,128)(2,1)} %get-tuple-element.18) | copy-start | bytes 393220
  186.5 2.9 %copy-start.17 = (f32[1024]{0:T(1024)S(1)}, f32[1024]{0:T(1024)}, u32[]{:S(2)}) copy-start(f32[1024]{0:T(1024)} %param.41) | copy-start | bytes 12292
  187.8 1.6 copy-start.8
  187.8 1.6 copy-start.12
Sparse Core Ops, SparseCore 0:
  90.4 15.4 all-gather.1
where the time goes:
time: 198 us; the launch traced here: 197 us
  blocking collectives  62.1 us (31%)
  waiting for transfers between devices  53.6 us (27%)
  local copies, waits for them, and re-layouts  26.5 us (13%)
  starting transfers between devices  17.7 us (9%)
  matrix products  17.6 us (9%)
  between operations  14.5 us (7%)
  other arithmetic  5.26 us (3%)
    all_to_all x1, blocking collectives, per_device(): lax.all_to_all(outgoing, 'ep', split_axis=0, concat_axis=0, tiled=True)  53.3 us
    all_to_all x1, waiting for transfers between devices, per_device(): lax.all_to_all(served, 'ep', split_axis=0, concat_axis=0, tiled=True)  36.2 us
    all_gather x1, waiting for transfers between devices, per_device(): lax.all_gather(lax.all_to_all(outgoing, 'ep', split_axis=0, concat_axis=0...  15.6 us
    all_to_all x1, starting transfers between devices, per_device(): lax.all_to_all(served, 'ep', split_axis=0, concat_axis=0, tiled=True)  10.8 us
    reshape x1, local copies, waits for them, and re-layouts, per_device(): taken_rows = incoming.reshape(source_count * slot_count, feature_count)  7.77 us
    all_to_all x2, starting transfers between devices, sent_to_all(): lax.all_to_all(jnp.broadcast_to(shard[None], (length, *shard.shape)), axi...  6.89 us
    all_to_all x1, blocking collectives, sent_to_all(): lax.all_to_all(jnp.broadcast_to(shard[None], (length, *shard.shape)), axi...  4.68 us
  transfers between devices with their start and end apart: 4, of which 4 were waited for; matrix products, arithmetic and copies ran while one was open for 2% of the time, Pallas kernels for 0%

commit v1 on v0

v1 whole, which is shorter than its diff:
```python
import jax
import jax.numpy as jnp
from jax import lax
from jax.experimental import pallas as pl
from jax.experimental.pallas import tpu as pltpu
from jax.sharding import PartitionSpec as P

BF = jnp.bfloat16
F32 = jnp.float32
MESH = pl.DeviceIdType.MESH

ROWS = 64
META = 8
BLOCK = ROWS + META
CUT = 40
HALF = 1024
LANES = ((0, 384), (384, 384), (768, 256))
ORDERS = ((0, 1, 2), (1, 2, 0), (2, 0, 1))
STRIDE = (16, 4, 1)
N_SEM = 256


def gathered_index(order, i, j):
    return (j, i) if order == 2 else (i, j)


def canonical(order, d, h):
    part = slice(None) if h is None else pl.ds(2 * h, 2)
    if order == 0:
        return (part, slice(None), d)
    if order == 1:
        return (d, part, slice(None))
    return (part, d, slice(None))


def power_of_two(exponent):
    value = jnp.ones(exponent.shape, F32)
    for bit in range(6):
        value = value * jnp.where((exponent >> bit) & 1 == 1, F32(2.0 ** (2**bit)), F32(1.0))
    return value


def dot(a, b):
    return jnp.dot(a, b, preferred_element_type=F32)


def dot_t(a, b):
    return lax.dot_general(a, b, (((0,), (0,)), ((), ())), preferred_element_type=F32)


def moe_kernel(
    n2, resid, ids_ref, wts_ref, scale_ref, eg, eu, ed, dg, du, dd,
    out,
    w_eg, w_eu, w_ed, w_dg, w_du, w_dd,
    ag0, ag1, ag2, cm0, cm1, cm2, ce0, ce1, ce2, fm0, fm1, fm2, fe0, fe1, fe2,
    xm, xe0, xe1, xe2, xx, hid, ym, yx, ye0, ye1, ye2,
    rm0, rm1, rm2, re0, re1, re2, gm0, gm1, gm2, ge0, ge1, ge2,
    pt0, pt1, pt2, sb0, sb1, sb2, rb0, rb1, rb2,
    pick_m, pick_e, comb_m, comb_e, dh, dense,
    ss, rs, ws,
):
    ag, cm, ce, fm, fe = (ag0, ag1, ag2), (cm0, cm1, cm2), (ce0, ce1, ce2), (fm0, fm1, fm2), (fe0, fe1, fe2)
    xe, ye, rm, re = (xe0, xe1, xe2), (ye0, ye1, ye2), (rm0, rm1, rm2), (re0, re1, re2)
    gm, ge, pt, sb, rb = (gm0, gm1, gm2), (ge0, ge1, ge2), (pt0, pt1, pt2), (sb0, sb1, sb2), (rb0, rb1, rb2)
    ep = lax.axis_index("ep")
    core = lax.axis_index("tp")
    coord = (ep // 16, (ep // 4) % 4, ep % 4)

    def along(axis, step):
        c = coord[axis]
        return ep + ((c + step) % 4 - c) * STRIDE[axis]

    next_dev = tuple((along(a, 1), core) for a in range(3))
    prev_dev = tuple((along(a, 3), core) for a in range(3))
    partner = (ep, 1 - core)

    barrier = pltpu.get_barrier_semaphore()
    for dev in (*next_dev, *prev_dev, partner):
        pl.semaphore_signal(barrier, inc=1, device_id=dev, device_id_type=MESH)

    loads = []

    def load(src, dst):
        copy = pltpu.make_async_copy(src, dst, ws.at[len(loads)])
        copy.start()
        loads.append(copy)

    own = pl.multiple_of(core * HALF, HALF)
    other = pl.multiple_of((1 - core) * HALF, HALF)
    own_h = pl.multiple_of(core * 256, 256)
    other_h = pl.multiple_of((1 - core) * 256, 256)
    for src, dst in ((dg, w_dg), (du, w_du)):
        load(src.at[pl.ds(own, HALF)], dst.at[0])
        load(src.at[pl.ds(other, HALF)], dst.at[1])
    load(dd.at[pl.ds(own_h, 256)], w_dd.at[0])
    load(dd.at[pl.ds(other_h, 256)], w_dd.at[1])
    for src, dst in ((eg, w_eg), (eu, w_eu)):
        load(src.at[0, pl.ds(own, HALF)], dst.at[0])
        load(src.at[0, pl.ds(other, HALF)], dst.at[1])
    load(ed.at[0, pl.ds(own_h, 256)], w_ed.at[0])
    load(ed.at[0, pl.ds(other_h, 256)], w_ed.at[1])

    used = [0]

    def remote(src, dst, dev):
        k = used[0]
        used[0] += 1
        return pltpu.make_async_remote_copy(
            src_ref=src, dst_ref=dst, send_sem=ss.at[k], recv_sem=rs.at[k], device_id=dev, device_id_type=MESH
        )

    sent = []

    def go(copy):
        copy.start()
        sent.append(copy)
        return copy

    lane = lax.broadcasted_iota(jnp.int32, (64, 128), 1)
    row = lax.broadcasted_iota(jnp.int32, (64, 128), 0)
    twice = (lane % 64 == row).astype(BF)
    ids_t = dot_t(ids_ref[...].astype(F32).astype(BF), twice)
    wts_t = dot_t(wts_ref[...].astype(BF), twice)
    experts = row.astype(F32)
    chosen = jnp.zeros((64, 128), F32)
    for k in range(6):
        chosen = chosen + jnp.where(ids_t[k : k + 1] == experts, F32(1.0), F32(0.0))
    earlier = ((lane % 64 > row)).astype(BF)
    rank = dot(chosen[:, :64].astype(BF), earlier)
    code = (rank + 32.0) * power_of_two(row)
    codes = [
        jnp.sum(jnp.where(ids_t[k : k + 1] == experts, code, F32(0.0)), axis=0, keepdims=True) for k in range(6)
    ]
    zeros2 = jnp.zeros((2, 128), F32)
    code8 = jnp.concatenate([*codes, zeros2], axis=0).astype(BF)
    wts8 = jnp.concatenate([wts_t, zeros2], axis=0).astype(BF)
    for o, (l0, w) in enumerate(LANES):
        ag[o][0, 0, 0:ROWS, :] = n2[0, :, l0 : l0 + w]
        ag[o][0, 0, ROWS:BLOCK, 0:128] = code8
        ag[o][0, 0, ROWS:BLOCK, 128:256] = wts8
        if w > 256:
            ag[o][0, 0, ROWS:BLOCK, 256:w] = jnp.zeros((META, w - 256), BF)

    pl.semaphore_wait(barrier, 7)

    def block(o, i, j, part=None):
        u, v = gathered_index(o, i, j)
        return ag[o].at[u, v] if part is None else ag[o].at[u, v, part]

    top, low = pl.ds(0, CUT), pl.ds(CUT, BLOCK - CUT)
    t1, t2, u1, u2 = {}, {}, {}, {}
    for o in range(3):
        a1, a2, _ = ORDERS[o]
        t1[o] = (
            go(remote(block(o, 0, 0), block(o, 3, 0), next_dev[a1])),
            go(remote(block(o, 0, 0), block(o, 1, 0), prev_dev[a1])),
        )

    def spread(o, i):
        a2 = ORDERS[o][1]
        u1[o, i] = (
            go(remote(block(o, i, 0), block(o, i, 3), next_dev[a2])),
            go(remote(block(o, i, 0), block(o, i, 1), prev_dev[a2])),
        )

    def relay(o, i):
        a2 = ORDERS[o][1]
        u1[o, i][0].wait_recv()
        u1[o, i][1].wait_recv()
        u2[o, i] = (
            go(remote(block(o, i, 3, top), block(o, i, 2, top), next_dev[a2])),
            go(remote(block(o, i, 1, low), block(o, i, 2, low), prev_dev[a2])),
        )

    for o in range(3):
        spread(o, 0)

    for h in range(2):
        for o in range(3):
            comb_m[o, h] = jnp.zeros((512, 512), BF)
            comb_e[o, h] = jnp.zeros((64, 512), BF)
    for b in range(2):
        pick_m[b] = jnp.zeros((512, 512), BF)

    for o in range(3):
        a1 = ORDERS[o][0]
        t1[o][0].wait_recv()
        t1[o][1].wait_recv()
        t2[o] = (
            go(remote(block(o, 3, 0, top), block(o, 2, 0, top), next_dev[a1])),
            go(remote(block(o, 1, 0, low), block(o, 2, 0, low), prev_dev[a1])),
        )
        spread(o, 3)
        spread(o, 1)
    for o in range(3):
        relay(o, 0)
    for o in range(3):
        t2[o][0].wait_recv()
        t2[o][1].wait_recv()
        spread(o, 2)
    for o in range(3):
        relay(o, 3)
        relay(o, 1)

    for copy in loads[:6]:
        copy.wait()
    n_own, n_other = n2[0], n2[1]
    d_gate = dot(n_own, w_dg[0]) + dot(n_other, w_dg[1])
    d_up = dot(n_own, w_du[0]) + dot(n_other, w_du[1])
    dh[0] = (jax.nn.silu(d_gate) * d_up).astype(BF)
    dh_copy = go(remote(dh.at[0], dh.at[1], partner))

    for o in range(3):
        relay(o, 2)
    dh_copy.wait_recv()
    dense[...] = (dot(dh[0], w_dd[0]) + dot(dh[1], w_dd[1])).astype(BF).astype(F32)

    lane128 = lax.broadcasted_iota(jnp.int32, (16, 128), 1)
    rank16 = lax.broadcasted_iota(jnp.int32, (16, 128), 0).astype(F32) + 32.0
    lane512 = lax.broadcasted_iota(jnp.int32, (16, 512), 1)
    row512 = lax.broadcasted_iota(jnp.int32, (16, 512), 0)
    extra_rank = (row512 % 2).astype(F32) + 48.0
    extra_own = lane512 // 64 == row512 // 2
    first_half = lax.broadcasted_iota(jnp.int32, (8, 128), 1) < 64
    arrived = {}

    def pick(o, h, buf):
        l0, w = LANES[o]
        a3 = ORDERS[o][2]
        code, weight = [], []
        for p in range(4):
            left = (2 * h + (2 * p) // 4, (2 * p) % 4)
            right = (2 * h + (2 * p + 1) // 4, (2 * p + 1) % 4)
            for into, at in ((code, 0), (weight, 128)):
                a = ag[o][left[0], left[1], ROWS:BLOCK, at : at + 128].astype(F32)
                b = ag[o][right[0], right[1], ROWS:BLOCK, at : at + 128].astype(F32)
                into.append(jnp.where(first_half, a, b))
        code = jnp.concatenate(code, axis=1)
        weight = jnp.concatenate(weight, axis=1)
        for d in range(4):
            scale = power_of_two(jnp.full((8, 512), along(a3, d), jnp.int32))
            mine = (code >= 32.0 * scale) & (code < 64.0 * scale)
            ranks = jnp.sum(jnp.where(mine, code, F32(0.0)), axis=0, keepdims=True)
            weights = jnp.sum(jnp.where(mine, weight, F32(0.0)), axis=0, keepdims=True)
            one = scale[0:1, 0:128]
            for s in range(8):
                lo = 128 * (s // 2)
                hit = (ranks[:, lo : lo + 128] == rank16 * one) & ((lane128 // 64) == s % 2)
                at = slice(128 * d + 16 * s, 128 * d + 16 * s + 16)
                pick_m[buf, at, lo : lo + 128] = jnp.where(hit, F32(1.0), F32(0.0)).astype(BF)
                comb_m[o, h, at, lo : lo + 128] = jnp.where(hit, weights[:, lo : lo + 128], F32(0.0)).astype(BF)
            hit = (ranks == extra_rank * scale[0:1]) & extra_own
            pick_e[buf, 16 * d : 16 * d + 16] = jnp.where(hit, F32(1.0), F32(0.0)).astype(BF)
            comb_e[o, h, 16 * d : 16 * d + 16] = jnp.where(hit, weights, F32(0.0)).astype(BF)
        rows = ag[o][2 * h : 2 * h + 2, :, 0:ROWS, :].reshape(512, w)
        main = dot(pick_m[buf], rows).astype(BF)
        extra = dot(pick_e[buf], rows).astype(BF)
        for d in range(4):
            m = main[128 * d : 128 * d + 128].reshape(2, 4, 16, w)
            e = extra[16 * d : 16 * d + 16]
            if d == 0:
                xm[(0, *canonical(o, 0, h), slice(None), pl.ds(l0, w))] = m
                xe[o][0, 0, h] = e
            else:
                cm[o][d - 1, h] = m
                ce[o][d - 1, h] = e
        ahead, behind = next_dev[a3], prev_dev[a3]
        far = ahead if h == 0 else behind
        into = lambda d: xm.at[(0, *canonical(o, d, h), slice(None), pl.ds(l0, w))]
        arrived[o, 2, h] = (
            go(remote(cm[o].at[1, h], fm[o].at[h], far)),
            go(remote(ce[o].at[1, h], fe[o].at[h], far)),
        )
        arrived[o, 3, h] = (
            go(remote(cm[o].at[0, h], into(3), ahead)),
            go(remote(ce[o].at[0, h], xe[o].at[0, 3, h], ahead)),
        )
        arrived[o, 1, h] = (
            go(remote(cm[o].at[2, h], into(1), behind)),
            go(remote(ce[o].at[2, h], xe[o].at[0, 1, h], behind)),
        )

    for o in range(3):
        for i in range(4):
            u2[o, i][0].wait_recv()
            u2[o, i][1].wait_recv()
        for h in range(2):
            pick(o, h, h)

    crossed = []

    def across(o, d):
        l0, w = LANES[o]
        at = (*canonical(o, d, None), slice(None), pl.ds(l0, w))
        crossed.append(go(remote(xm.at[(0, *at)], xm.at[(1, *at)], partner)))
        crossed.append(go(remote(xe[o].at[0, d], xe[o].at[1, d], partner)))

    for o in range(3):
        across(o, 0)
    for o in range(3):
        l0, w = LANES[o]
        a3 = ORDERS[o][2]
        for h in range(2):
            for copy in arrived[o, 2, h]:
                copy.wait_recv()
            far = next_dev[a3] if h == 0 else prev_dev[a3]
            arrived[o, 4, h] = (
                go(remote(fm[o].at[h], xm.at[(0, *canonical(o, 2, h), slice(None), pl.ds(l0, w))], far)),
                go(remote(fe[o].at[h], xe[o].at[0, 2, h], far)),
            )
    for d in (3, 1):
        for o in range(3):
            for h in range(2):
                for copy in arrived[o, d, h]:
                    copy.wait_recv()
            across(o, d)
    for o in range(3):
        for h in range(2):
            for copy in arrived[o, 4, h]:
                copy.wait_recv()
        across(o, 2)
    for copy in loads[6:]:
        copy.wait()
    for copy in crossed:
        copy.wait_recv()

    r128 = lax.broadcasted_iota(jnp.int32, (128, 128), 0)
    c128 = lax.broadcasted_iota(jnp.int32, (128, 128), 1)
    dz, dy, dx, bit = r128 // 32, (r128 // 8) % 4, (r128 // 2) % 4, r128 % 2
    turn = {
        0: (c128 == (dx * 16 + dz * 4 + dy) * 2 + bit).astype(BF),
        2: (c128 == (dy * 16 + dz * 4 + dx) * 2 + bit).astype(BF),
    }
    for c in range(2):
        for o, (l0, w) in enumerate(LANES):
            rows = xe[o][c].reshape(128, w)
            xx[c, :, l0 : l0 + w] = rows if o == 1 else dot(turn[o], rows).astype(BF)

    hid_copies = []
    for b in range(5):
        if b < 4:
            x_own, x_other = xm[0, b].reshape(256, HALF), xm[1, b].reshape(256, HALF)
        else:
            x_own, x_other = xx[0], xx[1]
        at = slice(256 * b, 256 * b + x_own.shape[0])
        gate = dot(x_own, w_eg[0]) + dot(x_other, w_eg[1])
        up = dot(x_own, w_eu[0]) + dot(x_other, w_eu[1])
        hid[0, at] = (jax.nn.silu(gate) * up).astype(BF)
        span = pl.ds(256 * b, x_own.shape[0])
        hid_copies.append(go(remote(hid.at[0, span], hid.at[1, span], partner)))
    for b in range(5):
        hid_copies[b].wait_recv()
        size = 256 if b < 4 else 128
        at = slice(256 * b, 256 * b + size)
        y = (dot(hid[0, at], w_ed[0]) + dot(hid[1, at], w_ed[1])).astype(BF)
        if b < 4:
            ym[b] = y.reshape(4, 4, 16, HALF)
        else:
            yx[...] = y
    for o, (l0, w) in enumerate(LANES):
        rows = yx[:, l0 : l0 + w]
        rows = rows if o == 1 else dot_t(turn[o], rows).astype(BF)
        ye[o][...] = rows.reshape(4, 2, 16, w)

    back = {}
    for o, (l0, w) in enumerate(LANES):
        a3 = ORDERS[o][2]
        ahead, behind = next_dev[a3], prev_dev[a3]
        part = lambda d, h: ym.at[(*canonical(o, d, h), slice(None), pl.ds(l0, w))]
        for h in range(2):
            far = ahead if h == 0 else behind
            back[o, 2, h] = (
                go(remote(part(2, h), gm[o].at[h], far)),
                go(remote(ye[o].at[2, h], ge[o].at[h], far)),
            )
        for h in range(2):
            back[o, 3, h] = (
                go(remote(part(1, h), rm[o].at[h, 3], ahead)),
                go(remote(ye[o].at[1, h], re[o].at[h, 3], ahead)),
            )
            back[o, 1, h] = (
                go(remote(part(3, h), rm[o].at[h, 1], behind)),
                go(remote(ye[o].at[3, h], re[o].at[h, 1], behind)),
            )
    for o, (l0, w) in enumerate(LANES):
        for h in range(2):
            rm[o][h, 0] = ym[(*canonical(o, 0, h), slice(None), pl.ds(l0, w))]
            re[o][h, 0] = ye[o][0, h]
    for o in range(3):
        a3 = ORDERS[o][2]
        for h in range(2):
            for copy in back[o, 2, h]:
                copy.wait_recv()
            far = next_dev[a3] if h == 0 else prev_dev[a3]
            back[o, 4, h] = (
                go(remote(gm[o].at[h], rm[o].at[h, 2], far)),
                go(remote(ge[o].at[h], re[o].at[h, 2], far)),
            )
    for o, (l0, w) in enumerate(LANES):
        for h in range(2):
            for d in (3, 1, 4):
                for copy in back[o, d, h]:
                    copy.wait_recv()
            part = dot_t(comb_m[o, h], rm[o][h].reshape(512, w)) + dot_t(comb_e[o, h], re[o][h].reshape(64, w))
            pt[o][2 * h : 2 * h + 2] = part.reshape(2, 4, ROWS, w)

    up32, low32 = slice(0, 32), slice(32, 64)
    stage_a, stage_b = {}, {}

    def at_sum(o, i, j):
        return (j, i) if o == 2 else (i, j)

    def start_far(o, n, axis, src):
        sb[o][n, 0] = pt[o][src].astype(BF)
        stage_a[o, n] = (
            go(remote(sb[o].at[n, 0, pl.ds(0, 32)], rb[o].at[n, 0, pl.ds(0, 32)], prev_dev[axis])),
            go(remote(sb[o].at[n, 0, pl.ds(32, 32)], rb[o].at[n, 0, pl.ds(32, 32)], next_dev[axis])),
        )

    def start_near(o, n, axis, third, first):
        stage_a[o, n][0].wait_recv()
        stage_a[o, n][1].wait_recv()
        sb[o][n, 1, 0:32] = (pt[o][(*third, up32)] + rb[o][n, 0, 0:32].astype(F32)).astype(BF)
        sb[o][n, 1, 32:64] = pt[o][(*third, low32)].astype(BF)
        sb[o][n, 2, 0:32] = pt[o][(*first, up32)].astype(BF)
        sb[o][n, 2, 32:64] = (pt[o][(*first, low32)] + rb[o][n, 0, 32:64].astype(F32)).astype(BF)
        stage_b[o, n] = (
            go(remote(sb[o].at[n, 1], rb[o].at[n, 1], prev_dev[axis])),
            go(remote(sb[o].at[n, 2], rb[o].at[n, 2], next_dev[axis])),
        )

    def finish(o, n, home):
        stage_b[o, n][0].wait_recv()
        stage_b[o, n][1].wait_recv()
        pt[o][home] = pt[o][home] + rb[o][n, 1].astype(F32) + rb[o][n, 2].astype(F32)

    for i in (2, 1, 3, 0):
        for o in range(3):
            start_far(o, i, ORDERS[o][1], at_sum(o, i, 2))
    for i in (2, 1, 3, 0):
        for o in range(3):
            start_near(o, i, ORDERS[o][1], at_sum(o, i, 3), at_sum(o, i, 1))
    for i in (2, 1, 3, 0):
        for o in range(3):
            finish(o, i, at_sum(o, i, 0))
            if i == 2:
                start_far(o, 4, ORDERS[o][0], at_sum(o, 2, 0))
            if i == 3:
                start_near(o, 4, ORDERS[o][0], at_sum(o, 3, 0), at_sum(o, 1, 0))
    for o, (l0, w) in enumerate(LANES):
        finish(o, 4, (0, 0))
        at = slice(l0, l0 + w)
        total = resid[:, at].astype(F32) + pt[o][0, 0] + scale_ref[:, at] * dense[:, at]
        out[:, at] = total.astype(BF)
    for copy in sent:
        copy.wait_send()


def moe(n2, resid, ids, wts, scale, eg, eu, ed, dg, du, dd):
    vmem = pl.BlockSpec(memory_space=pltpu.VMEM)
    anyspace = pl.BlockSpec(memory_space=pl.ANY)
    widths = [w for _, w in LANES]
    per = lambda f, dt=BF: [pltpu.VMEM(f(w), dt) for w in widths]
    scratch = [
        pltpu.VMEM((2, HALF, 256), BF), pltpu.VMEM((2, HALF, 256), BF), pltpu.VMEM((2, 256, HALF), BF),
        pltpu.VMEM((2, HALF, 256), BF), pltpu.VMEM((2, HALF, 256), BF), pltpu.VMEM((2, 256, HALF), BF),
        *per(lambda w: (4, 4, BLOCK, w)),
        *per(lambda w: (3, 2, 2, 4, 16, w)),
        *per(lambda w: (3, 2, 16, w)),
        *per(lambda w: (2, 2, 4, 16, w)),
        *per(lambda w: (2, 16, w)),
        pltpu.VMEM((2, 4, 4, 4, 16, HALF), BF),
        *per(lambda w: (2, 4, 2, 16, w)),
        pltpu.VMEM((2, 128, HALF), BF),
        pltpu.VMEM((2, 1152, 256), BF),
        pltpu.VMEM((4, 4, 4, 16, HALF), BF),
        pltpu.VMEM((128, HALF), BF),
        *per(lambda w: (4, 2, 16, w)),
        *per(lambda w: (2, 4, 2, 4, 16, w)),
        *per(lambda w: (2, 4, 16, w)),
        *per(lambda w: (2, 2, 4, 16, w)),
        *per(lambda w: (2, 16, w)),
        *per(lambda w: (4, 4, ROWS, w), F32),
        *per(lambda w: (5, 3, ROWS, w)),
        *per(lambda w: (5, 3, ROWS, w)),
        pltpu.VMEM((2, 512, 512), BF), pltpu.VMEM((2, 64, 512), BF),
        pltpu.VMEM((3, 2, 512, 512), BF), pltpu.VMEM((3, 2, 64, 512), BF),
        pltpu.VMEM((2, ROWS, 256), BF), pltpu.VMEM((ROWS, HALF), F32),
        pltpu.SemaphoreType.DMA((N_SEM,)), pltpu.SemaphoreType.DMA((N_SEM,)), pltpu.SemaphoreType.DMA((12,)),
    ]
    return pl.pallas_call(
        moe_kernel,
        out_shape=jax.ShapeDtypeStruct((ROWS, HALF), BF),
        in_specs=[vmem] * 5 + [anyspace] * 6,
        out_specs=vmem,
        scratch_shapes=scratch,
        compiler_params=pltpu.CompilerParams(
            collective_id=0, has_side_effects=True, vmem_limit_bytes=60 * 1024 * 1024
        ),
        name="moe",
    )(n2, resid, ids, wts, scale, eg, eu, ed, dg, du, dd)


def gathered_copies(shard, axis, dim):
    return lax.all_gather(shard, axis, axis=dim, tiled=True)


def normalize(part_rows, gain_vec):
    whole_rows = gathered_copies(part_rows, "tp", 1).astype(jnp.float32)
    row_mean = jnp.mean(whole_rows, axis=1, keepdims=True)
    row_var = jnp.mean(whole_rows * whole_rows, axis=1, keepdims=True) - row_mean * row_mean
    return ((whole_rows - row_mean) * lax.rsqrt(row_var + 1e-05) * gain_vec).astype(jnp.bfloat16)


def per_device(
    stream, conv_state, recur_state, mix_gain, branch_weight, gate_weight, conv_taps, recur_map, input_map,
    decay_logit, out_weight, moe_gain, route_ids, route_weights, expert_gate, expert_up, expert_down,
    dense_gate, dense_up, dense_down, dense_scale,
):
    seq_count = stream.shape[0]
    normed = normalize(stream, mix_gain)
    branch_in = jnp.dot(normed, branch_weight, preferred_element_type=jnp.float32).astype(jnp.bfloat16)
    gate_pre = jnp.dot(normed, gate_weight, preferred_element_type=jnp.float32).astype(jnp.bfloat16)
    conv_sum = branch_in.astype(jnp.float32) * conv_taps[3]
    for offset in range(3):
        conv_sum = conv_sum + conv_state[:, offset].astype(jnp.float32) * conv_taps[offset]
    conv_out = conv_sum.astype(jnp.bfloat16)
    new_conv = jnp.concatenate([conv_state[:, 1:], branch_in[:, None]], axis=1)
    grouped = conv_out.reshape(seq_count, recur_map.shape[0], recur_map.shape[1])
    recur_gate = jax.nn.sigmoid(
        jnp.einsum("nbc,bcd->nbd", grouped, recur_map, preferred_element_type=jnp.float32)
    ).reshape(seq_count, -1)
    input_gate = jax.nn.sigmoid(
        jnp.einsum("nbc,bcd->nbd", grouped, input_map, preferred_element_type=jnp.float32)
    ).reshape(seq_count, -1)
    log_decay = -8.0 * recur_gate * jax.nn.softplus(-decay_logit)
    driven = jnp.sqrt(-jnp.expm1(2.0 * log_decay)) * (input_gate * conv_out.astype(jnp.float32))
    new_state = jnp.exp(log_decay) * recur_state + driven
    mixer_in = (jax.nn.gelu(gate_pre.astype(jnp.float32)) * new_state).astype(jnp.bfloat16)
    mixer_out = dot(lax.all_gather(mixer_in, "tp", axis=1, tiled=True), out_weight).astype(jnp.bfloat16)
    resid = (stream.astype(jnp.float32) + mixer_out.astype(jnp.float32)).astype(jnp.bfloat16)
    normed_two = normalize(resid, moe_gain)
    core = lax.axis_index("tp")
    n2 = jnp.stack(
        [
            lax.dynamic_slice_in_dim(normed_two, core * HALF, HALF, 1),
            lax.dynamic_slice_in_dim(normed_two, (1 - core) * HALF, HALF, 1),
        ]
    )
    result = moe(
        n2, resid, route_ids, route_weights, dense_scale.reshape(1, HALF),
        expert_gate, expert_up, expert_down, dense_gate, dense_up, dense_down,
    )
    return (result, new_state, new_conv)


def solution(mesh):
    in_specs = (
        P("ep", "tp"), P("ep", None, "tp"), P("ep", "tp"), P(), P(None, "tp"), P(None, "tp"), P(None, "tp"),
        P("tp", None, None), P("tp", None, None), P("tp"), P(None, "tp"), P(), P("ep", None), P("ep", None),
        P("ep", None, "tp"), P("ep", None, "tp"), P("ep", None, "tp"), P(None, "tp"), P(None, "tp"),
        P(None, "tp"), P("tp"),
    )
    out_specs = (P("ep", "tp"), P("ep", "tp"), P("ep", None, "tp"))
    return jax.shard_map(per_device, mesh=mesh, in_specs=in_specs, out_specs=out_specs, check_vma=False)
```

time: 198 us -> 97.2 us (0.49)
  Pallas kernels: 0 us -> 77.6 us
  blocking collectives: 62.1 us -> 6.51 us
  waiting for transfers between devices: 53.6 us -> 0 us
  local copies, waits for them, and re-layouts: 26.5 us -> 3.98 us
  starting transfers between devices: 17.7 us -> 0 us
  between operations: 14.5 us -> 0.9 us
  matrix products: 17.6 us -> 5.65 us
  other arithmetic: 5.26 us -> 2.28 us
    pallas_call x0 -> x1, Pallas kernels: none -> 77.6 us  [moe(): pl.pallas_call(moe_kernel, out_shape=jax.ShapeDtypeStruct((ROWS, HALF), B...]
    all_to_all x2 -> x0, blocking collectives: 58 us -> none  [the longest x1 53.3 us: per_device(): lax.all_to_all(outgoing, 'ep', split_axis=0, concat_axis=0, tiled=True)]
    all_to_all x3 -> x0, waiting for transfers between devices: 37.9 us -> none  [the longest x1 36.2 us: per_device(): lax.all_to_all(served, 'ep', split_axis=0, concat_axis=0, tiled=True)]
    all_to_all x3 -> x0, starting transfers between devices: 17.6 us -> none  [the longest x1 10.8 us: per_device(): lax.all_to_all(served, 'ep', split_axis=0, concat_axis=0, tiled=True)]
    all_gather x1 -> x0, waiting for transfers between devices: 15.6 us -> none  [per_device(): lax.all_gather(lax.all_to_all(outgoing, 'ep', split_axis=0, concat_axis=0...]
    reshape x4 -> x0, local copies, waits for them, and re-layouts: 15.6 us -> none  [the longest x1 7.77 us: per_device(): taken_rows = incoming.reshape(source_count * slot_count, feature_count)]
    dot_general x8 -> x1, matrix products: 12.2 us -> 0.86 us  [dot(): return jnp.dot(a, b, preferred_element_type=F32)]
    reduce_sum x3 -> x0, other arithmetic: 2.69 us -> none  [the longest x1 1.57 us: per_device(): jnp.sum(picked.astype(jnp.float32) * route_weights[:, :, None], axis=1)]
  transfers between devices with their start and end apart: 4 -> 0, of which waited for: 4 -> 0; matrix products, arithmetic and copies ran while one was open for 2% -> 0% of each run, Pallas kernels for 0% -> 0%
where the time goes in v1:
time: 97.2 us; the launch traced here: 96.9 us
  Pallas kernels  77.6 us (80%)
  blocking collectives  6.51 us (7%)
  matrix products  5.65 us (6%)
  local copies, waits for them, and re-layouts  3.98 us (4%)
  other arithmetic  2.28 us (2%)
    pallas_call x1, Pallas kernels, moe(): pl.pallas_call(moe_kernel, out_shape=jax.ShapeDtypeStruct((ROWS, HALF), B...  77.6 us
    all_gather x2, blocking collectives, gathered_copies(): return lax.all_gather(shard, axis, axis=dim, tiled=True)  4.51 us
    dot_general x1, matrix products, per_device(): jnp.dot(normed, branch_weight, preferred_element_type=jnp.float32)  3.36 us
    unnamed x29, local copies, waits for them, and re-layouts  3.06 us
    all_gather x1, blocking collectives, per_device(): lax.all_gather(mixer_in, 'tp', axis=1, tiled=True)  1.99 us

profile of v1, /device:TPU:0, one launch (start us, length us, event | category | flops | bytes accessed | tf_op | source)
XLA Modules:
  0.0 96.9 jit_solution(1194136407711345744)
XLA Ops:
  0.6 0.0 copy-start
  0.6 0.0 copy-start.12
  0.7 0.0 copy-start.11
  0.7 0.0 copy-start.6
  0.7 2.3 %all_gather.9 = bf16[64,2048]{1,0:T(8,128)(2,1)S(1)} all-gather(bf16[64,1024]{1,0:T(8,128)(2,1)} %param.21), channel_id=1, replica_groups=mesh['ep'=64,'tp'=2] {'tp'}, dimensions={1}, use_global_device_ids=true | all-gather | bytes 393216 | tf_op jit(solution)/shard_map/all_gather | solution.py:505
  3.0 0.2 convert_reduce_fusion.1
  3.2 0.9 fusion.42
  4.1 0.0 copy-start.2
  4.1 0.0 copy-start.7
  4.1 3.4 %fusion.32 = (bf16[64,1024]{1,0:T(8,128)(2,1)S(1)}, bf16[64,1024]{1,0:T(8,128)(2,1)S(1)}) fusion(f32[1024]{0:T(1024)S(1)} %bitcast.56, bf16[64,3,1024]{2,0,1:T(8,128)(2,1)} %param.22, f32[1024]{0:T(1024)S(1)} %bitcast.57, f32[1024]{0:T(1024)S(1)} %bitcast.55, f32[1024]{0:T(1024)S(1)} %bitcast.54, bf16[2048,1024]{1,0:T(8,128)(2,1)} %param.25, ...), kind=kOutput, calls=%fused_computation.49 | convolution fusion | flops 269942784 | bytes 5136896 | tf_op jit(solution)/shard_map/dot_general | solution.py:522
  7.5 0.0 copy-done
  7.5 0.2 fusion.3
  7.7 0.0 copy-done.12
  7.7 0.0 copy-start.1
  7.7 0.0 copy-start.5
  7.8 0.2 fusion.7
  8.0 0.0 copy-done.11
  8.0 0.0 copy-done.6
  8.0 0.2 fusion.30
  8.3 0.0 copy-done.2
  8.3 0.0 copy-done.7
  8.3 0.0 copy-start.4
  8.3 0.0 copy-start.8
  8.3 1.0 fusion.28
  9.3 0.0 copy-start.9
  9.3 0.0 copy-start.10
  9.3 2.0 %all_gather.10 = bf16[64,2048]{1,0:T(8,128)(2,1)S(1)} all-gather(bf16[64,1024]{1,0:T(8,128)(2,1)S(1)} %fusion.28), channel_id=1, replica_groups=mesh['ep'=64,'tp'=2] {'tp'}, dimensions={1}, use_global_device_ids=true | all-gather | bytes 393216 | tf_op jit(solution)/shard_map/all_gather | solution.py:540
  11.3 0.0 copy-done.1
  11.3 0.0 copy-done.5
  11.3 0.9 fusion.10.resid
  12.2 0.0 copy-done.4
  12.2 0.0 copy-start.3
  12.2 2.2 %all_gather.11 = bf16[64,2048]{1,0:T(8,128)(2,1)S(1)} all-gather(bf16[64,1024]{1,0:T(8,128)(2,1)S(1)} %fusion.10.resid), channel_id=1, replica_groups=mesh['ep'=64,'tp'=2] {'tp'}, dimensions={1}, use_global_device_ids=true | all-gather | bytes 393216 | tf_op jit(solution)/shard_map/all_gather | solution.py:505
  14.4 0.2 convert_reduce_fusion
  14.6 0.0 copy-done.8
  14.6 0.2 fusion.18
  14.7 0.0 slice-start
  14.8 0.7 pad_maximum_fusion.1.n2
  15.5 0.0 copy-done.9
  15.5 0.7 copy.28.ids_ref
  16.2 0.0 copy-done.10
  16.2 0.7 copy.29.wts_ref
  16.9 0.0 copy-done.3
  16.9 77.6 %moe.1 = bf16[64,1024]{1,0:T(8,128)(2,1)} custom-call(bf16[2,64,1024]{2,1,0:T(8,128)(2,1)} %pad_maximum_fusion.1.n2, bf16[64,1024]{1,0:T(8,128)(2,1)} %copy-done.3, s32[64,6]{1,0:T(8,128)} %copy.28.ids_ref, f32[64,6]{1,0:T(8,128)} %copy.29.wts_ref, f32[1,1024]{1,0:T(1,128)} %bitcast.58, bf16[1,2048,256]{2,1,0:T(8,128)(2,1)} %eg.1, bf16[1,2048,256]{2,1,0:T(8,128)(2,1)} %eu.1, ...), custom_call_target="tpu_custom_call" | custom-call | tf_op jit(solution)/shard_map/moe/pallas_call | solution.py:491
  94.6 0.0 slice-done
  94.6 0.8 pad_maximum_fusion
  95.4 1.6 %copy.46 = bf16[64,1024]{1,0:T(8,128)(2,1)} copy(bf16[64,1024]{1,0:T(8,128)(2,1)} %moe.1) | data formatting | bytes 262144
  (4 shorter events, 0.1 us)
Async XLA Ops:
  0.6 6.9 %copy-start = (bf16[8,128,128]{2,1,0:T(8,128)(2,1)S(1)}, bf16[8,128,128]{2,1,0:T(8,128)(2,1)}, u32[]{:S(2)}) copy-start(bf16[8,128,128]{2,1,0:T(8,128)(2,1)} %param.29) | copy-start | bytes 786436
  0.6 7.1 %copy-start.12 = (bf16[8,128,128]{2,1,0:T(8,128)(2,1)S(1)}, bf16[8,128,128]{2,1,0:T(8,128)(2,1)}, u32[]{:S(2)}) copy-start(bf16[8,128,128]{2,1,0:T(8,128)(2,1)} %param.28) | copy-start | bytes 786436
  0.7 7.3 %copy-start.11 = (f32[1024]{0:T(1024)S(1)}, f32[1024]{0:T(1024)}, u32[]{:S(2)}) copy-start(f32[1024]{0:T(1024)} %param.30) | copy-start | bytes 12292
  0.7 7.4 %copy-start.6 = (f32[64,1024]{1,0:T(8,128)S(1)}, f32[64,1024]{1,0:T(8,128)}, u32[]{:S(2)}) copy-start(f32[64,1024]{1,0:T(8,128)} %param.23) | copy-start | bytes 786436
  4.1 4.2 %copy-start.2 = (bf16[2048,1024]{1,0:T(8,128)(2,1)S(1)}, bf16[2048,1024]{1,0:T(8,128)(2,1)}, u32[]{:S(2)}) copy-start(bf16[2048,1024]{1,0:T(8,128)(2,1)} %param.26) | copy-start | bytes 12582916
  4.1 4.2 %copy-start.7 = (f32[2048]{0:T(1024)S(1)}, f32[2048]{0:T(1024)}, u32[]{:S(2)}) copy-start(f32[2048]{0:T(1024)} %param.24) | copy-start | bytes 24580
  7.7 3.6 %copy-start.1 = (bf16[2048,1024]{1,0:T(8,128)(2,1)S(1)}, bf16[2048,1024]{1,0:T(8,128)(2,1)}, u32[]{:S(2)}) copy-start(bf16[2048,1024]{1,0:T(8,128)(2,1)} %param.31) | copy-start | bytes 12582916
  7.7 3.6 %copy-start.5 = (bf16[64,1024]{1,0:T(8,128)(2,1)S(1)}, bf16[64,1024]{1,0:T(8,128)(2,1)}, u32[]{:S(2)}) copy-start(bf16[64,1024]{1,0:T(8,128)(2,1)} %param.21) | copy-start | bytes 393220
  8.3 3.9 %copy-start.4 = (f32[64,1024]{1,0:T(8,128)}, f32[64,1024]{1,0:T(8,128)S(1)}, u32[]{:S(2)}) copy-start(f32[64,1024]{1,0:T(8,128)S(1)} %fusion.30) | copy-start | bytes 786436
  8.3 6.3 %copy-start.8 = (f32[2048]{0:T(1024)S(1)}, f32[2048]{0:T(1024)}, u32[]{:S(2)}) copy-start(f32[2048]{0:T(1024)} %param.32) | copy-start | bytes 24580
  9.3 6.2 %copy-start.9 = (s32[64,6]{0,1:T(8,128)S(1)}, s32[64,6]{0,1:T(8,128)}, u32[]{:S(2)}) copy-start(s32[64,6]{0,1:T(8,128)} %param.33) | copy-start | bytes 4612
  9.3 6.9 %copy-start.10 = (f32[64,6]{0,1:T(8,128)S(1)}, f32[64,6]{0,1:T(8,128)}, u32[]{:S(2)}) copy-start(f32[64,6]{0,1:T(8,128)} %param.34) | copy-start | bytes 4612
  12.2 4.8 %copy-start.3 = (bf16[64,1024]{1,0:T(8,128)(2,1)}, bf16[64,1024]{1,0:T(8,128)(2,1)S(1)}, u32[]{:S(2)}) copy-start(bf16[64,1024]{1,0:T(8,128)(2,1)S(1)} %fusion.10.resid) | copy-start | bytes 393220
  14.7 79.8 %slice-start = ((bf16[64,3,1024]{2,0,1:T(8,128)(2,1)}), bf16[64,2,1024]{2,0,1:T(8,128)(2,1)S(1)}, s32[]{:S(2)}) async-start(bf16[64,3,1024]{2,0,1:T(8,128)(2,1)} %param.22), calls=%async_computation | async-start | bytes 524288 | tf_op jit(solution)/shard_map/slice | solution.py:528

commit v2 on v1

v2 whole, which is shorter than its diff:
```python
import jax
import jax.numpy as jnp
from jax import lax
from jax.experimental import pallas as pl
from jax.experimental.pallas import tpu as pltpu
from jax.sharding import PartitionSpec as P

BF = jnp.bfloat16
F32 = jnp.float32
MESH = pl.DeviceIdType.MESH

ROWS = 64
META = 8
BLOCK = ROWS + META
CUT = 40
HALF = 1024
LANES = ((0, 384), (384, 384), (768, 256))
ORDERS = ((0, 1, 2), (1, 2, 0), (2, 0, 1))
STRIDE = (16, 4, 1)
N_SEM = 320


ALL = slice(None)


def arranged(order, i, j):
    return (j, i) if order == 2 else (i, j)


def canonical(order, d, i):
    if order == 0:
        return (i, ALL, d)
    if order == 1:
        return (d, i, ALL)
    return (ALL, d, i)


def pair(h):
    return pl.ds(2 * h, 2)


def power_of_two(exponent):
    value = jnp.ones(exponent.shape, F32)
    for bit in range(6):
        value = value * jnp.where((exponent >> bit) & 1 == 1, F32(2.0 ** (2**bit)), F32(1.0))
    return value


def dot(a, b):
    return jnp.dot(a, b, preferred_element_type=F32)


def dot_t(a, b):
    return lax.dot_general(a, b, (((0,), (0,)), ((), ())), preferred_element_type=F32)


def layer_kernel(
    stream, ids_ref, wts_ref, mix_gain, moe_gain, taps, decay, scale_ref, conv_hbm, state_hbm, rmap_hbm, imap_hbm,
    wb, wg, wo, eg, eu, ed, dg, du, dd,
    rest, resid_out, branch_out, kept_out, driven_out,
    w_b, w_g, w_o, w_eg, w_eu, w_ed, w_dg, w_du, w_dd, conv_in, state_in, w_r, w_i, st, mi, r2, n2,
    ag0, ag1, ag2, cm0, cm1, cm2, ce0, ce1, ce2, fm0, fm1, fm2, fe0, fe1, fe2,
    xm, xe0, xe1, xe2, xx, hid, ym, yx, ye0, ye1, ye2,
    rm0, rm1, rm2, re0, re1, re2, gm0, gm1, gm2, ge0, ge1, ge2,
    pt0, pt1, pt2, sb0, sb1, sb2, rb0, rb1, rb2,
    pick_m, pick_e, comb_m, comb_e, dh, dense,
    ss, rs, ws,
):
    ag, cm, ce, fm, fe = (ag0, ag1, ag2), (cm0, cm1, cm2), (ce0, ce1, ce2), (fm0, fm1, fm2), (fe0, fe1, fe2)
    xe, ye, rm, re = (xe0, xe1, xe2), (ye0, ye1, ye2), (rm0, rm1, rm2), (re0, re1, re2)
    gm, ge, pt, sb, rb = (gm0, gm1, gm2), (ge0, ge1, ge2), (pt0, pt1, pt2), (sb0, sb1, sb2), (rb0, rb1, rb2)
    ep = lax.axis_index("ep")
    core = lax.axis_index("tp")
    coord = (ep // 16, (ep // 4) % 4, ep % 4)

    def along(axis, step):
        c = coord[axis]
        return ep + ((c + step) % 4 - c) * STRIDE[axis]

    next_dev = tuple((along(a, 1), core) for a in range(3))
    prev_dev = tuple((along(a, 3), core) for a in range(3))
    partner = (ep, 1 - core)

    barrier = pltpu.get_barrier_semaphore()
    for dev in (*next_dev, *prev_dev, partner):
        pl.semaphore_signal(barrier, inc=1, device_id=dev, device_id_type=MESH)

    loads = [0]

    def load(*copies):
        started = []
        for src, dst in copies:
            copy = pltpu.make_async_copy(src, dst, ws.at[loads[0]])
            loads[0] += 1
            copy.start()
            started.append(copy)
        return started

    def halves(src, dst, size):
        own = pl.multiple_of(core * size, size)
        other = pl.multiple_of((1 - core) * size, size)
        return (src.at[pl.ds(own, size)], dst.at[0]), (src.at[pl.ds(other, size)], dst.at[1])

    def landed(copies):
        for copy in copies:
            copy.wait()

    branch_load = load(*halves(wb, w_b, HALF))
    gate_load = load(
        (conv_hbm, conv_in), (rmap_hbm, w_r), (imap_hbm, w_i), (state_hbm, state_in), *halves(wg, w_g, HALF)
    )
    out_load = load(*halves(wo, w_o, HALF))

    used = [0]

    def remote(src, dst, dev):
        k = used[0]
        used[0] += 1
        return pltpu.make_async_remote_copy(
            src_ref=src, dst_ref=dst, send_sem=ss.at[k], recv_sem=rs.at[k], device_id=dev, device_id_type=MESH
        )

    sent = []

    def go(copy):
        copy.start()
        sent.append(copy)
        return copy

    lane = lax.broadcasted_iota(jnp.int32, (64, 128), 1)
    row = lax.broadcasted_iota(jnp.int32, (64, 128), 0)
    twice = (lane % 64 == row).astype(BF)
    ids_t = dot(ids_ref[...].astype(F32).astype(BF), twice)
    wts_t = dot(wts_ref[...].astype(BF), twice)
    experts = row.astype(F32)
    chosen = jnp.zeros((64, 128), F32)
    for k in range(6):
        chosen = chosen + jnp.where(ids_t[k : k + 1] == experts, F32(1.0), F32(0.0))
    earlier = (lane % 64 > row).astype(BF)
    rank = dot(chosen[:, :64].astype(BF), earlier)
    code = (rank + 32.0) * power_of_two(row)
    codes = [
        jnp.sum(jnp.where(ids_t[k : k + 1] == experts, code, F32(0.0)), axis=0, keepdims=True) for k in range(6)
    ]
    zeros2 = jnp.zeros((2, 128), F32)
    code8 = jnp.concatenate([*codes, zeros2], axis=0).astype(BF)
    wts8 = jnp.concatenate([wts_t, zeros2], axis=0).astype(BF)
    for o, (l0, w) in enumerate(LANES):
        ag[o][0, 0, ROWS:BLOCK, 0:128] = code8
        ag[o][0, 0, ROWS:BLOCK, 128:256] = wts8
        if w > 256:
            ag[o][0, 0, ROWS:BLOCK, 256:w] = jnp.zeros((META, w - 256), BF)
    for h in range(2):
        for o in range(3):
            comb_m[o, h] = jnp.zeros((512, 512), BF)
    for b in range(2):
        pick_m[b] = jnp.zeros((512, 512), BF)

    pl.semaphore_wait(barrier, 7)

    own_lanes = pl.ds(pl.multiple_of(core * HALF, HALF), HALF)
    other_lanes = pl.ds(pl.multiple_of((1 - core) * HALF, HALF), HALF)
    stream_copy = go(remote(stream, st, partner))
    shift = -decay[...]
    rate = -8.0 * (jnp.maximum(shift, 0.0) + jnp.log1p(jnp.exp(-jnp.abs(shift))))
    stream_copy.wait_recv()

    def normed(own_ref, other_ref, gain):
        a, b = own_ref.astype(F32), other_ref.astype(F32)
        total = jnp.sum(a, axis=1, keepdims=True) + jnp.sum(b, axis=1, keepdims=True)
        square = jnp.sum(a * a, axis=1, keepdims=True) + jnp.sum(b * b, axis=1, keepdims=True)
        mean = total * (1.0 / 2048)
        inv = lax.rsqrt(square * (1.0 / 2048) - mean * mean + 1e-05)
        return (
            ((a - mean) * inv * gain[:, own_lanes]).astype(BF),
            ((b - mean) * inv * gain[:, other_lanes]).astype(BF),
        )

    n_own, n_other = normed(stream[...], st[...], mix_gain)
    landed(branch_load)
    branch = (dot(n_own, w_b[0]) + dot(n_other, w_b[1])).astype(BF)
    branch_out[...] = branch
    landed(gate_load)
    late_load = load(*halves(dg, w_dg, HALF), *halves(du, w_du, HALF), *halves(dd, w_dd, 256))
    gate_pre = (dot(n_own, w_g[0]) + dot(n_other, w_g[1])).astype(BF)
    mixed = branch.astype(F32) * taps[3:4]
    for k in range(3):
        mixed = mixed + conv_in[k].astype(F32) * taps[k : k + 1]
    conv_out = mixed.astype(BF)
    for b in range(8):
        at = slice(128 * b, 128 * b + 128)
        piece = conv_out[:, at]
        recur_gate = jax.nn.sigmoid(dot(piece, w_r[b]))
        input_gate = jax.nn.sigmoid(dot(piece, w_i[b]))
        log_decay = recur_gate * rate[:, at]
        decayed = jnp.exp(log_decay)
        gap = jnp.tanh(-log_decay) * (1.0 + decayed * decayed)
        driven = jnp.sqrt(gap) * (input_gate * piece.astype(F32))
        kept = decayed * state_in[:, at]
        kept_out[:, at] = kept
        driven_out[:, at] = driven
        mi[0, :, at] = (jax.nn.gelu(gate_pre[:, at].astype(F32)) * (kept + driven)).astype(BF)
    mixer_copy = go(remote(mi.at[0], mi.at[1], partner))
    landed(out_load)
    expert_load = load(
        *halves(eg.at[0], w_eg, HALF), *halves(eu.at[0], w_eu, HALF), *halves(ed.at[0], w_ed, 256)
    )
    partial = dot(mi[0], w_o[0])
    mixer_copy.wait_recv()
    mixer_out = (partial + dot(mi[1], w_o[1])).astype(BF)
    r2[0] = (stream[...].astype(F32) + mixer_out.astype(F32)).astype(BF)
    resid_copy = go(remote(r2.at[0], r2.at[1], partner))
    resid_out[...] = r2[0]
    resid_copy.wait_recv()
    n_own, n_other = normed(r2[0], r2[1], moe_gain)
    n2[0] = n_own
    n2[1] = n_other
    for o, (l0, w) in enumerate(LANES):
        ag[o][0, 0, 0:ROWS, :] = n_own[:, l0 : l0 + w]

    def block(o, i, j, part=None):
        return ag[o].at[i, j] if part is None else ag[o].at[i, j, part]

    top, low = pl.ds(0, CUT), pl.ds(CUT, BLOCK - CUT)
    t1, t2, u1, u2 = {}, {}, {}, {}
    for o in range(3):
        a1 = ORDERS[o][0]
        t1[o] = (
            go(remote(block(o, 0, 0), block(o, 3, 0), next_dev[a1])),
            go(remote(block(o, 0, 0), block(o, 1, 0), prev_dev[a1])),
        )

    def spread(o, i):
        a2 = ORDERS[o][1]
        u1[o, i] = (
            go(remote(block(o, i, 0), block(o, i, 3), next_dev[a2])),
            go(remote(block(o, i, 0), block(o, i, 1), prev_dev[a2])),
        )

    def relay(o, i):
        a2 = ORDERS[o][1]
        u1[o, i][0].wait_recv()
        u1[o, i][1].wait_recv()
        u2[o, i] = (
            go(remote(block(o, i, 3, top), block(o, i, 2, top), next_dev[a2])),
            go(remote(block(o, i, 1, low), block(o, i, 2, low), prev_dev[a2])),
        )

    def relayed(o, i):
        u2[o, i][0].wait_recv()
        u2[o, i][1].wait_recv()

    for o in range(3):
        spread(o, 0)

    landed(late_load)
    d_gate = dot(n_own, w_dg[0]) + dot(n_other, w_dg[1])
    d_up = dot(n_own, w_du[0]) + dot(n_other, w_du[1])
    dh[0] = (jax.nn.silu(d_gate) * d_up).astype(BF)
    dh_copy = go(remote(dh.at[0], dh.at[1], partner))

    for o in range(3):
        a1 = ORDERS[o][0]
        t1[o][0].wait_recv()
        t1[o][1].wait_recv()
        t2[o] = (
            go(remote(block(o, 3, 0, top), block(o, 2, 0, top), next_dev[a1])),
            go(remote(block(o, 1, 0, low), block(o, 2, 0, low), prev_dev[a1])),
        )
    for o in range(3):
        spread(o, 1)
        spread(o, 3)
    for o in range(3):
        relay(o, 0)
    for o in range(3):
        t2[o][0].wait_recv()
        t2[o][1].wait_recv()
        spread(o, 2)
    for o in range(3):
        relay(o, 1)
    for o in range(3):
        relay(o, 3)
    for o in range(3):
        relay(o, 2)
    dh_copy.wait_recv()
    dense[...] = (dot(dh[0], w_dd[0]) + dot(dh[1], w_dd[1])).astype(BF).astype(F32)

    lane128 = lax.broadcasted_iota(jnp.int32, (16, 128), 1)
    rank16 = lax.broadcasted_iota(jnp.int32, (16, 128), 0).astype(F32) + 32.0
    lane512 = lax.broadcasted_iota(jnp.int32, (16, 512), 1)
    row512 = lax.broadcasted_iota(jnp.int32, (16, 512), 0)
    extra_rank = (row512 % 2).astype(F32) + 48.0
    extra_own = lane512 // 64 == row512 // 2
    first_half = lax.broadcasted_iota(jnp.int32, (8, 128), 1) < 64
    arrived = {}

    def pick(o, h, buf):
        l0, w = LANES[o]
        a3 = ORDERS[o][2]
        code, weight = [], []
        for p in range(4):
            i, j = 2 * h + p // 2, (2 * p) % 4
            for into, at in ((code, 0), (weight, 128)):
                a = ag[o][i, j, ROWS:BLOCK, at : at + 128].astype(F32)
                b = ag[o][i, j + 1, ROWS:BLOCK, at : at + 128].astype(F32)
                into.append(jnp.where(first_half, a, b))
        code = jnp.concatenate(code, axis=1)
        weight = jnp.concatenate(weight, axis=1)
        for d in range(4):
            scale = power_of_two(jnp.full((8, 512), along(a3, d), jnp.int32))
            mine = (code >= 32.0 * scale) & (code < 64.0 * scale)
            ranks = jnp.sum(jnp.where(mine, code, F32(0.0)), axis=0, keepdims=True)
            weights = jnp.sum(jnp.where(mine, weight, F32(0.0)), axis=0, keepdims=True)
            one = scale[0:1, 0:128]
            for s in range(8):
                lo = 128 * (s // 2)
                hit = (ranks[:, lo : lo + 128] == rank16 * one) & ((lane128 // 64) == s % 2)
                at = 128 * d + 16 * s
                pick_m[buf, at : at + 16, lo : lo + 128] = jnp.where(hit, F32(1.0), F32(0.0)).astype(BF)
                back_at = 128 * d + 16 * ((s % 4) * 2 + s // 4) if o == 2 else at
                comb_m[o, h, back_at : back_at + 16, lo : lo + 128] = jnp.where(
                    hit, weights[:, lo : lo + 128], F32(0.0)
                ).astype(BF)
            hit = (ranks == extra_rank * scale[0:1]) & extra_own
            pick_e[buf, 16 * d : 16 * d + 16] = jnp.where(hit, F32(1.0), F32(0.0)).astype(BF)
            comb_e[o, h, 16 * d : 16 * d + 16] = jnp.where(hit, weights, F32(0.0)).astype(BF)
        rows = ag[o][2 * h : 2 * h + 2, :, 0:ROWS, :].reshape(512, w)
        main = dot(pick_m[buf], rows).astype(BF)
        extra = dot(pick_e[buf], rows).astype(BF)
        for d in range(4):
            e = extra[16 * d : 16 * d + 16]
            for ii in range(2):
                at = 128 * d + 64 * ii
                m = main[at : at + 64].reshape(4, 16, w)
                if d == 0:
                    xm[(0, *canonical(o, 0, 2 * h + ii), ALL, pl.ds(l0, w))] = m
                else:
                    cm[o][(d - 1, *arranged(o, 2 * h + ii, ALL))] = m
            if d == 0:
                xe[o][0, 0, h] = e
            else:
                ce[o][d - 1, h] = e
        ahead, behind = next_dev[a3], prev_dev[a3]
        for ii in range(2):
            i = 2 * h + ii
            far = ahead if ii == 0 else behind
            arrived[o, 2, i] = (
                go(remote(cm[o].at[(1, *arranged(o, i, ALL))], fm[o].at[i], far)),
                go(remote(ce[o].at[1, h, pl.ds(8 * ii, 8)], fe[o].at[i], far)),
            )

    def direct(o, h):
        l0, w = LANES[o]
        a3 = ORDERS[o][2]
        ahead, behind = next_dev[a3], prev_dev[a3]
        into = lambda d: xm.at[(0, *canonical(o, d, pair(h)), ALL, pl.ds(l0, w))]
        arrived[o, 3, h] = (
            go(remote(cm[o].at[(0, *arranged(o, pair(h), ALL))], into(3), ahead)),
            go(remote(ce[o].at[0, h], xe[o].at[0, 3, h], ahead)),
        )
        arrived[o, 1, h] = (
            go(remote(cm[o].at[(2, *arranged(o, pair(h), ALL))], into(1), behind)),
            go(remote(ce[o].at[2, h], xe[o].at[0, 1, h], behind)),
        )

    def pass_on(o, h):
        l0, w = LANES[o]
        a3 = ORDERS[o][2]
        for ii in range(2):
            i = 2 * h + ii
            for copy in arrived[o, 2, i]:
                copy.wait_recv()
            far = next_dev[a3] if ii == 0 else prev_dev[a3]
            arrived[o, 4, i] = (
                go(remote(fm[o].at[i], xm.at[(0, *canonical(o, 2, i), ALL, pl.ds(l0, w))], far)),
                go(remote(fe[o].at[i], xe[o].at[0, 2, h, pl.ds(8 * ii, 8)], far)),
            )

    crossed = []

    def across(o, d):
        l0, w = LANES[o]
        at = (*canonical(o, d, ALL), ALL, pl.ds(l0, w))
        crossed.append(go(remote(xm.at[(0, *at)], xm.at[(1, *at)], partner)))
        crossed.append(go(remote(xe[o].at[0, d], xe[o].at[1, d], partner)))

    for o in range(3):
        relayed(o, 0)
        relayed(o, 1)
        pick(o, 0, 0)
    for o in range(3):
        direct(o, 0)
    for o in range(3):
        relayed(o, 2)
        relayed(o, 3)
        pick(o, 1, 1)
    for o in range(3):
        across(o, 0)
    for o in range(3):
        pass_on(o, 0)
    for o in range(3):
        direct(o, 1)
    for o in range(3):
        pass_on(o, 1)
    for o in range(3):
        for d in (3, 1):
            for h in range(2):
                for copy in arrived[o, d, h]:
                    copy.wait_recv()
            across(o, d)
    for o in range(3):
        for i in range(4):
            for copy in arrived[o, 4, i]:
                copy.wait_recv()
        across(o, 2)
    landed(expert_load)
    for copy in crossed:
        copy.wait_recv()

    r128 = lax.broadcasted_iota(jnp.int32, (128, 128), 0)
    c128 = lax.broadcasted_iota(jnp.int32, (128, 128), 1)
    dz, dy, dx, bit = r128 // 32, (r128 // 8) % 4, (r128 // 2) % 4, r128 % 2
    turn = {
        0: (c128 == (dx * 16 + dz * 4 + dy) * 2 + bit).astype(BF),
        2: (c128 == (dy * 16 + dx * 4 + dz) * 2 + bit).astype(BF),
    }
    for c in range(2):
        for o, (l0, w) in enumerate(LANES):
            rows = xe[o][c].reshape(128, w)
            xx[c, :, l0 : l0 + w] = rows if o == 1 else dot(turn[o], rows).astype(BF)

    hid_copies = []
    for b in range(5):
        if b < 4:
            x_own, x_other = xm[0, b].reshape(256, HALF), xm[1, b].reshape(256, HALF)
        else:
            x_own, x_other = xx[0], xx[1]
        at = slice(256 * b, 256 * b + x_own.shape[0])
        gate = dot(x_own, w_eg[0]) + dot(x_other, w_eg[1])
        up = dot(x_own, w_eu[0]) + dot(x_other, w_eu[1])
        hid[0, at] = (jax.nn.silu(gate) * up).astype(BF)
        span = pl.ds(256 * b, x_own.shape[0])
        hid_copies.append(go(remote(hid.at[0, span], hid.at[1, span], partner)))
    for b in range(5):
        hid_copies[b].wait_recv()
        size = 256 if b < 4 else 128
        at = slice(256 * b, 256 * b + size)
        y = (dot(hid[0, at], w_ed[0]) + dot(hid[1, at], w_ed[1])).astype(BF)
        if b < 4:
            ym[b] = y.reshape(4, 4, 16, HALF)
        else:
            yx[...] = y
    for o, (l0, w) in enumerate(LANES):
        rows = yx[:, l0 : l0 + w]
        rows = rows if o == 1 else dot_t(turn[o], rows).astype(BF)
        ye[o][...] = rows.reshape(4, 2, 16, w)

    back = {}

    def part(o, d, i):
        l0, w = LANES[o]
        return ym.at[(*canonical(o, d, i), ALL, pl.ds(l0, w))]

    def slots(o, h, d, ii=None):
        if ii is None:
            return rm[o].at[h, d]
        return rm[o].at[(h, d, *arranged(o, ii, ALL))]

    for h in (1, 0):
        for o in range(3):
            a3 = ORDERS[o][2]
            for ii in range(2):
                far = next_dev[a3] if ii == 0 else prev_dev[a3]
                i = 2 * h + ii
                back[o, 2, i] = (
                    go(remote(part(o, 2, i), gm[o].at[i], far)),
                    go(remote(ye[o].at[2, h, pl.ds(8 * ii, 8)], ge[o].at[i], far)),
                )

    def direct_back(h):
        for o in range(3):
            a3 = ORDERS[o][2]
            back[o, 3, h] = (
                go(remote(part(o, 1, pair(h)), slots(o, h, 3), next_dev[a3])),
                go(remote(ye[o].at[1, h], re[o].at[h, 3], next_dev[a3])),
            )
            back[o, 1, h] = (
                go(remote(part(o, 3, pair(h)), slots(o, h, 1), prev_dev[a3])),
                go(remote(ye[o].at[3, h], re[o].at[h, 1], prev_dev[a3])),
            )

    direct_back(1)
    for o, (l0, w) in enumerate(LANES):
        for h in range(2):
            rm[o][h, 0] = ym[(*canonical(o, 0, slice(2 * h, 2 * h + 2)), ALL, slice(l0, l0 + w))]
            re[o][h, 0] = ye[o][0, h]

    def pass_back(h):
        for o in range(3):
            a3 = ORDERS[o][2]
            for ii in range(2):
                i = 2 * h + ii
                for copy in back[o, 2, i]:
                    copy.wait_recv()
                far = next_dev[a3] if ii == 0 else prev_dev[a3]
                back[o, 4, i] = (
                    go(remote(gm[o].at[i], slots(o, h, 2, ii), far)),
                    go(remote(ge[o].at[i], re[o].at[h, 2, pl.ds(8 * ii, 8)], far)),
                )

    def combine(o, h):
        w = LANES[o][1]
        for key in ((o, 3, h), (o, 1, h), (o, 4, 2 * h), (o, 4, 2 * h + 1)):
            for copy in back[key]:
                copy.wait_recv()
        sums = dot_t(comb_m[o, h], rm[o][h].reshape(512, w)) + dot_t(comb_e[o, h], re[o][h].reshape(64, w))
        pt[o][2 * h : 2 * h + 2] = sums.reshape(2, 4, ROWS, w)

    up32, low32 = slice(0, 32), slice(32, 64)
    stage_a, stage_b = {}, {}

    def start_far(o, n, axis, src):
        sb[o][n, 0] = pt[o][src].astype(BF)
        stage_a[o, n] = (
            go(remote(sb[o].at[n, 0, pl.ds(0, 32)], rb[o].at[n, 0, pl.ds(0, 32)], prev_dev[axis])),
            go(remote(sb[o].at[n, 0, pl.ds(32, 32)], rb[o].at[n, 0, pl.ds(32, 32)], next_dev[axis])),
        )

    def start_near(o, n, axis, third, first):
        stage_a[o, n][0].wait_recv()
        stage_a[o, n][1].wait_recv()
        sb[o][n, 1, 0:32] = (pt[o][(*third, up32)] + rb[o][n, 0, 0:32].astype(F32)).astype(BF)
        sb[o][n, 1, 32:64] = pt[o][(*third, low32)].astype(BF)
        sb[o][n, 2, 0:32] = pt[o][(*first, up32)].astype(BF)
        sb[o][n, 2, 32:64] = (pt[o][(*first, low32)] + rb[o][n, 0, 32:64].astype(F32)).astype(BF)
        stage_b[o, n] = (
            go(remote(sb[o].at[n, 1], rb[o].at[n, 1], prev_dev[axis])),
            go(remote(sb[o].at[n, 2], rb[o].at[n, 2], next_dev[axis])),
        )

    def finish(o, n, home):
        stage_b[o, n][0].wait_recv()
        stage_b[o, n][1].wait_recv()
        pt[o][home] = pt[o][home] + rb[o][n, 1].astype(F32) + rb[o][n, 2].astype(F32)

    def far(i):
        for o in range(3):
            start_far(o, i, ORDERS[o][1], (i, 2))

    def near(i):
        for o in range(3):
            start_near(o, i, ORDERS[o][1], (i, 3), (i, 1))

    pass_back(1)
    pass_back(0)
    direct_back(0)
    for o in range(3):
        combine(o, 1)
        for i in (2, 3):
            start_far(o, i, ORDERS[o][1], (i, 2))
    near(2)
    near(3)
    for o in range(3):
        combine(o, 0)
        for i in (1, 0):
            start_far(o, i, ORDERS[o][1], (i, 2))
    for o in range(3):
        finish(o, 2, (2, 0))
        start_far(o, 4, ORDERS[o][0], (2, 0))
    near(1)
    near(0)
    for o in range(3):
        finish(o, 3, (3, 0))
        finish(o, 1, (1, 0))
        start_near(o, 4, ORDERS[o][0], (3, 0), (1, 0))
    for o in range(3):
        finish(o, 0, (0, 0))
    for o, (l0, w) in enumerate(LANES):
        finish(o, 4, (0, 0))
        at = slice(l0, l0 + w)
        rest[:, at] = pt[o][0, 0] + scale_ref[:, at] * dense[:, at]
    for copy in sent:
        copy.wait_send()


def layer(*args):
    vmem = pl.BlockSpec(memory_space=pltpu.VMEM)
    anyspace = pl.BlockSpec(memory_space=pl.ANY)
    widths = [w for _, w in LANES]
    per = lambda f, dt=BF: [pltpu.VMEM(f(w), dt) for w in widths]
    duo = lambda o: (4, 2) if o == 2 else (2, 4)
    scratch = [
        *[pltpu.VMEM((2, HALF, HALF), BF)] * 3,
        pltpu.VMEM((2, HALF, 256), BF), pltpu.VMEM((2, HALF, 256), BF), pltpu.VMEM((2, 256, HALF), BF),
        pltpu.VMEM((2, HALF, 256), BF), pltpu.VMEM((2, HALF, 256), BF), pltpu.VMEM((2, 256, HALF), BF),
        pltpu.VMEM((3, ROWS, HALF), BF), pltpu.VMEM((ROWS, HALF), F32),
        pltpu.VMEM((8, 128, 128), BF), pltpu.VMEM((8, 128, 128), BF),
        pltpu.VMEM((ROWS, HALF), BF),
        *[pltpu.VMEM((2, ROWS, HALF), BF)] * 3,
        *per(lambda w: (4, 4, BLOCK, w)),
        *per(lambda w: (3, 4, 4, 16, w)),
        *per(lambda w: (3, 2, 16, w)),
        *per(lambda w: (4, 4, 16, w)),
        *per(lambda w: (4, 8, w)),
        pltpu.VMEM((2, 4, 4, 4, 16, HALF), BF),
        *per(lambda w: (2, 4, 2, 16, w)),
        pltpu.VMEM((2, 128, HALF), BF),
        pltpu.VMEM((2, 1152, 256), BF),
        pltpu.VMEM((4, 4, 4, 16, HALF), BF),
        pltpu.VMEM((128, HALF), BF),
        *per(lambda w: (4, 2, 16, w)),
        *[pltpu.VMEM((2, 4, *duo(o), 16, w), BF) for o, w in enumerate(widths)],
        *per(lambda w: (2, 4, 16, w)),
        *per(lambda w: (4, 4, 16, w)),
        *per(lambda w: (4, 8, w)),
        *per(lambda w: (4, 4, ROWS, w), F32),
        *per(lambda w: (5, 3, ROWS, w)),
        *per(lambda w: (5, 3, ROWS, w)),
        pltpu.VMEM((2, 512, 512), BF), pltpu.VMEM((2, 64, 512), BF),
        pltpu.VMEM((3, 2, 512, 512), BF), pltpu.VMEM((3, 2, 64, 512), BF),
        pltpu.VMEM((2, ROWS, 256), BF), pltpu.VMEM((ROWS, HALF), F32),
        pltpu.SemaphoreType.DMA((N_SEM,)), pltpu.SemaphoreType.DMA((N_SEM,)), pltpu.SemaphoreType.DMA((24,)),
    ]
    wide = jax.ShapeDtypeStruct((ROWS, HALF), F32)
    short = jax.ShapeDtypeStruct((ROWS, HALF), BF)
    return pl.pallas_call(
        layer_kernel,
        out_shape=(wide, short, short, wide, wide),
        in_specs=[vmem] * 8 + [anyspace] * 13,
        out_specs=(vmem,) * 5,
        scratch_shapes=scratch,
        compiler_params=pltpu.CompilerParams(
            collective_id=0, has_side_effects=True, vmem_limit_bytes=58 * 1024 * 1024
        ),
        name="layer",
    )(*args)


def outputs_kernel(conv_hbm, rest, resid, branch, kept, driven, result, state, conv, r_buf, s_buf, c_buf, sems):
    old = pltpu.make_async_copy(conv_hbm.at[pl.ds(1, 2)], c_buf, sems.at[0])
    old.start()
    last = pltpu.make_async_copy(branch, conv.at[2], sems.at[1])
    last.start()
    s_buf[...] = kept[...] + driven[...]
    state_copy = pltpu.make_async_copy(s_buf, state, sems.at[2])
    state_copy.start()
    r_buf[...] = (resid[...].astype(F32) + rest[...]).astype(BF)
    result_copy = pltpu.make_async_copy(r_buf, result, sems.at[3])
    result_copy.start()
    old.wait()
    moved = pltpu.make_async_copy(c_buf, conv.at[pl.ds(0, 2)], sems.at[4])
    moved.start()
    for copy in (last, state_copy, result_copy, moved):
        copy.wait()


def outputs(*args):
    vmem = pl.BlockSpec(memory_space=pltpu.VMEM)
    anyspace = pl.BlockSpec(memory_space=pl.ANY)
    return pl.pallas_call(
        outputs_kernel,
        out_shape=(
            jax.ShapeDtypeStruct((ROWS, HALF), BF),
            jax.ShapeDtypeStruct((ROWS, HALF), F32),
            jax.ShapeDtypeStruct((3, ROWS, HALF), BF),
        ),
        in_specs=[anyspace] + [vmem] * 5,
        out_specs=(anyspace,) * 3,
        scratch_shapes=[
            pltpu.VMEM((ROWS, HALF), BF), pltpu.VMEM((ROWS, HALF), F32), pltpu.VMEM((2, ROWS, HALF), BF),
            pltpu.SemaphoreType.DMA((5,)),
        ],
        name="outputs",
    )(*args)


def per_device(
    stream, conv_state, recur_state, mix_gain, branch_weight, gate_weight, conv_taps, recur_map, input_map,
    decay_logit, out_weight, moe_gain, route_ids, route_weights, expert_gate, expert_up, expert_down,
    dense_gate, dense_up, dense_down, dense_scale,
):
    conv_turned = jnp.transpose(conv_state, (1, 0, 2))
    parts = layer(
        stream, route_ids.T, route_weights.T, mix_gain.reshape(1, -1), moe_gain.reshape(1, -1), conv_taps,
        decay_logit.reshape(1, -1), dense_scale.reshape(1, -1), conv_turned, recur_state,
        recur_map, input_map, branch_weight, gate_weight, out_weight,
        expert_gate, expert_up, expert_down, dense_gate, dense_up, dense_down,
    )
    result, new_state, new_conv = outputs(conv_turned, *parts)
    return (result, new_state, jnp.transpose(new_conv, (1, 0, 2)))


def solution(mesh):
    in_specs = (
        P("ep", "tp"), P("ep", None, "tp"), P("ep", "tp"), P(), P(None, "tp"), P(None, "tp"), P(None, "tp"),
        P("tp", None, None), P("tp", None, None), P("tp"), P(None, "tp"), P(), P("ep", None), P("ep", None),
        P("ep", None, "tp"), P("ep", None, "tp"), P("ep", None, "tp"), P(None, "tp"), P(None, "tp"),
        P(None, "tp"), P("tp"),
    )
    out_specs = (P("ep", "tp"), P("ep", "tp"), P("ep", None, "tp"))
    return jax.shard_map(per_device, mesh=mesh, in_specs=in_specs, out_specs=out_specs, check_vma=False)
```

time: 97.2 us -> 85.4 us (0.88)
  Pallas kernels: 77.6 us -> 84.4 us
  blocking collectives: 6.51 us -> 0 us
  matrix products: 5.65 us -> 0 us
  local copies, waits for them, and re-layouts: 3.98 us -> 0 us
  other arithmetic: 2.28 us -> 0 us
    pallas_call x1 -> x2, Pallas kernels: 77.6 us -> 84.4 us  [the longest x1 81.3 us: layer(): pl.pallas_call(layer_kernel, out_shape=(wide, short, short, wide, wide),...]
    all_gather x3 -> x0, blocking collectives: 6.51 us -> none  [the longest x2 4.51 us: gathered_copies(): return lax.all_gather(shard, axis, axis=dim, tiled=True)]
    dot_general x5 -> x0, matrix products: 5.65 us -> none  [the longest x1 3.36 us: per_device(): jnp.dot(normed, branch_weight, preferred_element_type=jnp.float32)]
    unnamed x29 -> x0, local copies, waits for them, and re-layouts: 3.06 us -> none
where the time goes in v2:
time: 85.4 us; the launch traced here: 85.2 us
  Pallas kernels  84.4 us (99%)
    pallas_call x1, Pallas kernels, layer(): pl.pallas_call(layer_kernel, out_shape=(wide, short, short, wide, wide),...  81.3 us
    pallas_call x1, Pallas kernels, outputs(): pl.pallas_call(outputs_kernel, out_shape=(jax.ShapeDtypeStruct((ROWS, HAL...  3.06 us

profile of v2, /device:TPU:0, one launch (start us, length us, event | category | flops | bytes accessed | tf_op | source)
XLA Modules:
  0.0 85.2 jit_solution(13242344567868767710)
XLA Ops:
  0.6 81.3 %layer.1 = (f32[64,1024]{1,0:T(8,128)}, bf16[64,1024]{1,0:T(8,128)(2,1)}, bf16[64,1024]{1,0:T(8,128)(2,1)}, f32[64,1024]{1,0:T(8,128)}, f32[64,1024]{1,0:T(8,128)}) custom-call(bf16[64,1024]{1,0:T(8,128)(2,1)} %stream.1, s32[6,64]{1,0:T(8,128)} %bitcast.12, f32[6,64]{1,0:T(8,128)} %bitcast.13, f32[1,2048]{1,0:T(1,128)} %bitcast.10, f32[1,2048]{1,0:T(1,128)} %bitcast.11, ...), custom_call_target="tpu_custom_call" | custom-call | tf_op jit(solution)/shard_map/layer/pallas_call | solution.py:626
  82.0 3.1 %outputs.1 = (bf16[64,1024]{1,0:T(8,128)(2,1)}, f32[64,1024]{1,0:T(8,128)}, bf16[3,64,1024]{2,1,0:T(8,128)(2,1)}) custom-call(bf16[3,64,1024]{2,1,0:T(8,128)(2,1)} %bitcast.9, f32[64,1024]{1,0:T(8,128)} %get-tuple-element.11.rest, bf16[64,1024]{1,0:T(8,128)(2,1)} %get-tuple-element.12.resid, bf16[64,1024]{1,0:T(8,128)(2,1)} %get-tuple-element.13.branch, ...), custom_call_target="tpu_custom_call" | custom-call | tf_op jit(solution)/shard_map/outputs/pallas_call | solution.py:660

commit v3 on v2

v3 whole, which is shorter than its diff:
```python
import jax
import jax.numpy as jnp
from jax import lax
from jax.experimental import pallas as pl
from jax.experimental.pallas import tpu as pltpu
from jax.sharding import PartitionSpec as P

BF = jnp.bfloat16
F32 = jnp.float32
MESH = pl.DeviceIdType.MESH
ALL = slice(None)

ROWS = 64
META = 8
BLOCK = ROWS + META
CUT = 40
HALF = 1024
LANES = ((0, 384), (384, 384), (768, 256))
ORDERS = ((0, 1, 2), (1, 2, 0), (2, 0, 1))
STRIDE = (16, 4, 1)
SLOTS = 48
NEAR = (0, 1, 3)


def canonical(order, d, i):
    if order == 0:
        return (i, ALL, d)
    if order == 1:
        return (d, i, ALL)
    return (ALL, d, i)


def power_of_two(exponent):
    value = jnp.ones(exponent.shape, F32)
    for bit in range(6):
        value = value * jnp.where((exponent >> bit) & 1 == 1, F32(2.0 ** (2**bit)), F32(1.0))
    return value


def dot(a, b):
    return jnp.dot(a, b, preferred_element_type=F32)


def dot_t(a, b):
    return lax.dot_general(a, b, (((0,), (0,)), ((), ())), preferred_element_type=F32)


def layer_kernel(
    stream_hbm, ids_hbm, wts_hbm, mix_gain_hbm, moe_gain_hbm, taps_hbm, decay_hbm, scale_hbm, conv_hbm, state_hbm,
    rmap_hbm, imap_hbm, wb, wg, wo, eg, eu, ed, dg, du, dd,
    rest, resid_out, branch_out, kept_out, driven_out,
    stream, ids_ref, wts_ref, mix_gain, moe_gain, taps, decay, scale_ref,
    w_b, w_g, w_o, w_eg, w_eu, w_ed, w_dg, w_du, w_dd, conv_in, state_in, w_r, w_i, st, mi, r2,
    ag0, ag1, ag2, cm0, cm1, cm2, ce0, ce1, ce2, fm0, fm1, fm2, fe0, fe1, fe2,
    xm, xe0, xe1, xe2, xx, hid, ym, yx, ye0, ye1, ye2,
    rm0, rm1, rm2, gm0, gm1, gm2, ge0, ge1, ge2,
    pt0, pt1, pt2, sb0, sb1, sb2, rb0, rb1, rb2,
    pick_m, comb_m, dh, dense,
    ss, rs, ws,
):
    ag, cm, ce, fm, fe = (ag0, ag1, ag2), (cm0, cm1, cm2), (ce0, ce1, ce2), (fm0, fm1, fm2), (fe0, fe1, fe2)
    xe, ye, rm = (xe0, xe1, xe2), (ye0, ye1, ye2), (rm0, rm1, rm2)
    gm, ge, pt, sb, rb = (gm0, gm1, gm2), (ge0, ge1, ge2), (pt0, pt1, pt2), (sb0, sb1, sb2), (rb0, rb1, rb2)
    ep = lax.axis_index("ep")
    core = lax.axis_index("tp")
    coord = (ep // 16, (ep // 4) % 4, ep % 4)

    def along(axis, step):
        c = coord[axis]
        return ep + ((c + step) % 4 - c) * STRIDE[axis]

    next_dev = tuple((along(a, 1), core) for a in range(3))
    prev_dev = tuple((along(a, 3), core) for a in range(3))
    partner = (ep, 1 - core)

    barrier = pltpu.get_barrier_semaphore()
    for dev in (*next_dev, *prev_dev, partner):
        pl.semaphore_signal(barrier, inc=1, device_id=dev, device_id_type=MESH)

    n_load = [0]

    def whole(src, dst):
        k = n_load[0]
        n_load[0] += 1
        copy = pltpu.make_async_copy(src, dst, ws.at[k])
        copy.start()
        return copy

    def halves(src, dst, size):
        k = n_load[0]
        n_load[0] += 1
        own = pl.multiple_of(core * size, size)
        other = pl.multiple_of((1 - core) * size, size)
        pltpu.make_async_copy(src.at[pl.ds(own, size)], dst.at[0], ws.at[k]).start()
        pltpu.make_async_copy(src.at[pl.ds(other, size)], dst.at[1], ws.at[k]).start()
        return pltpu.make_async_copy(dst, dst, ws.at[k])

    def landed(*copies):
        for copy in copies:
            copy.wait()

    ids_load, wts_load, stream_load = whole(ids_hbm, ids_ref), whole(wts_hbm, wts_ref), whole(stream_hbm, stream)
    small_load = (
        whole(mix_gain_hbm, mix_gain), whole(decay_hbm, decay), whole(taps_hbm, taps),
    )
    branch_load = halves(wb, w_b, HALF)
    gate_load = (
        whole(conv_hbm, conv_in), whole(rmap_hbm, w_r), whole(imap_hbm, w_i), whole(state_hbm, state_in),
        halves(wg, w_g, HALF),
    )
    out_load = halves(wo, w_o, HALF)
    norm_load = (whole(moe_gain_hbm, moe_gain), whole(scale_hbm, scale_ref))

    sends = []

    def go(tag, ref, dev, *pairs):
        k = len(sends)
        if k >= SLOTS:
            sends[k - SLOTS].wait()
        send_sem = ss.at[k % SLOTS]
        for src, dst in pairs:
            pltpu.make_async_remote_copy(
                src_ref=src, dst_ref=dst, send_sem=send_sem, recv_sem=rs.at[tag], device_id=dev, device_id_type=MESH
            ).start()
        sends.append(pltpu.make_async_copy(ref, ref, send_sem))

    def take(tag, ref):
        pltpu.make_async_copy(ref, ref, rs.at[tag]).wait()

    T1, T2, U1, U2 = 0, 3, 6, 18
    SUM_A, SUM_B = 0, 15
    FAR, DIRECT, PASSED = 30, 42, 54
    BACK_FAR, BACK = 66, 78
    CROSS, EXTRA, ROW = 90, 93, 94
    HIDDEN = 98

    for k in range(12):
        comb_m[k] = jnp.zeros((288, 256), BF)
    for b in range(3):
        pick_m[b] = jnp.zeros((288, 256), BF)
    lane = lax.broadcasted_iota(jnp.int32, (64, 128), 1)
    row = lax.broadcasted_iota(jnp.int32, (64, 128), 0)
    twice = (lane % 64 == row).astype(BF)
    landed(ids_load, wts_load)
    ids_t = dot(ids_ref[...].astype(F32).astype(BF), twice)
    wts_t = dot(wts_ref[...].astype(BF), twice)
    experts = row.astype(F32)
    chosen = jnp.zeros((64, 128), F32)
    for k in range(6):
        chosen = chosen + jnp.where(ids_t[k : k + 1] == experts, F32(1.0), F32(0.0))
    earlier = (lane % 64 > row).astype(BF)
    rank = dot(chosen[:, :64].astype(BF), earlier)
    code = (rank + 32.0) * power_of_two(row)
    codes = [
        jnp.sum(jnp.where(ids_t[k : k + 1] == experts, code, F32(0.0)), axis=0, keepdims=True) for k in range(6)
    ]
    zeros2 = jnp.zeros((2, 128), F32)
    code8 = jnp.concatenate([*codes, zeros2], axis=0).astype(BF)
    wts8 = jnp.concatenate([wts_t, zeros2], axis=0).astype(BF)
    for o, (l0, w) in enumerate(LANES):
        ag[o][0, 0, ROWS:BLOCK, 0:128] = code8
        ag[o][0, 0, ROWS:BLOCK, 128:256] = wts8
        if w > 256:
            ag[o][0, 0, ROWS:BLOCK, 256:w] = jnp.zeros((META, w - 256), BF)

    landed(stream_load)
    pl.semaphore_wait(barrier, 7)

    own_lanes = pl.ds(pl.multiple_of(core * HALF, HALF), HALF)
    other_lanes = pl.ds(pl.multiple_of((1 - core) * HALF, HALF), HALF)
    go(ROW, stream, partner, (stream, st))
    landed(*small_load)
    shift = -decay[...]
    rate = -8.0 * (jnp.maximum(shift, 0.0) + jnp.log1p(jnp.exp(-jnp.abs(shift))))
    take(ROW, st)

    def normed(own_ref, other_ref, gain):
        a, b = own_ref.astype(F32), other_ref.astype(F32)
        total = jnp.sum(a, axis=1, keepdims=True) + jnp.sum(b, axis=1, keepdims=True)
        square = jnp.sum(a * a, axis=1, keepdims=True) + jnp.sum(b * b, axis=1, keepdims=True)
        mean = total * (1.0 / 2048)
        inv = lax.rsqrt(square * (1.0 / 2048) - mean * mean + 1e-05)
        return (
            ((a - mean) * inv * gain[:, own_lanes]).astype(BF),
            ((b - mean) * inv * gain[:, other_lanes]).astype(BF),
        )

    n_own, n_other = normed(stream[...], st[...], mix_gain)
    landed(branch_load)
    branch = (dot(n_own, w_b[0]) + dot(n_other, w_b[1])).astype(BF)
    branch_out[...] = branch
    landed(*gate_load)
    dense_load = (halves(dg, w_dg, HALF), halves(du, w_du, HALF), halves(dd, w_dd, 256))
    gate_pre = (dot(n_own, w_g[0]) + dot(n_other, w_g[1])).astype(BF)
    mixed = branch.astype(F32) * taps[3:4]
    for k in range(3):
        mixed = mixed + conv_in[k].astype(F32) * taps[k : k + 1]
    conv_out = mixed.astype(BF)
    for b in range(8):
        at = slice(128 * b, 128 * b + 128)
        piece = conv_out[:, at]
        recur_gate = jax.nn.sigmoid(dot(piece, w_r[b]))
        input_gate = jax.nn.sigmoid(dot(piece, w_i[b]))
        log_decay = recur_gate * rate[:, at]
        decayed = jnp.exp(log_decay)
        gap = jnp.tanh(-log_decay) * (1.0 + decayed * decayed)
        driven = jnp.sqrt(gap) * (input_gate * piece.astype(F32))
        kept = decayed * state_in[:, at]
        kept_out[:, at] = kept
        driven_out[:, at] = driven
        mi[0, :, at] = (jax.nn.gelu(gate_pre[:, at].astype(F32)) * (kept + driven)).astype(BF)
    go(ROW + 1, mi.at[0], partner, (mi.at[0], mi.at[1]))
    landed(out_load)
    expert_load = (
        halves(eg.at[0], w_eg, HALF), halves(eu.at[0], w_eu, HALF), halves(ed.at[0], w_ed, 256),
    )
    partial = dot(mi[0], w_o[0])
    take(ROW + 1, mi.at[1])
    mixer_out = (partial + dot(mi[1], w_o[1])).astype(BF)
    r2[0] = (stream[...].astype(F32) + mixer_out.astype(F32)).astype(BF)
    go(ROW + 2, r2.at[0], partner, (r2.at[0], r2.at[1]))
    resid_out[...] = r2[0]
    landed(*norm_load)
    take(ROW + 2, r2.at[1])
    n_own, n_other = normed(r2[0], r2[1], moe_gain)
    for o, (l0, w) in enumerate(LANES):
        ag[o][0, 0, 0:ROWS, :] = n_own[:, l0 : l0 + w]

    def block(o, i, j, part=None):
        return ag[o].at[i, j] if part is None else ag[o].at[i, j, part]

    def one(o):
        return ag[o].at[0, 0]

    def two(o):
        return ag[o].at[0, pl.ds(0, 2)]

    def three(o):
        return ag[o].at[0, pl.ds(0, 3)]

    top, low = pl.ds(0, CUT), pl.ds(CUT, BLOCK - CUT)

    def spread(o, i):
        a2 = ORDERS[o][1]
        go(U1 + 4 * o + i, one(o), next_dev[a2], (block(o, i, 0), block(o, i, 3)))
        go(U1 + 4 * o + i, one(o), prev_dev[a2], (block(o, i, 0), block(o, i, 1)))

    def relay(o, i):
        a2 = ORDERS[o][1]
        take(U1 + 4 * o + i, two(o))
        tag = U2 + 4 * o + i
        go(tag, block(o, i, 2, top), next_dev[a2], (block(o, i, 3, top), block(o, i, 2, top)))
        go(tag, block(o, i, 2, low), prev_dev[a2], (block(o, i, 1, low), block(o, i, 2, low)))

    def relayed(o, i):
        take(U2 + 4 * o + i, one(o))

    for o in range(3):
        a1 = ORDERS[o][0]
        go(T1 + o, one(o), next_dev[a1], (block(o, 0, 0), block(o, 3, 0)))
        go(T1 + o, one(o), prev_dev[a1], (block(o, 0, 0), block(o, 1, 0)))
    for o in range(3):
        spread(o, 0)

    landed(*dense_load)
    d_gate = dot(n_own, w_dg[0]) + dot(n_other, w_dg[1])
    d_up = dot(n_own, w_du[0]) + dot(n_other, w_du[1])
    dh[0] = (jax.nn.silu(d_gate) * d_up).astype(BF)
    go(ROW + 3, dh.at[0], partner, (dh.at[0], dh.at[1]))

    for o in range(3):
        a1 = ORDERS[o][0]
        take(T1 + o, two(o))
        go(T2 + o, block(o, 2, 0, top), next_dev[a1], (block(o, 3, 0, top), block(o, 2, 0, top)))
        go(T2 + o, block(o, 2, 0, low), prev_dev[a1], (block(o, 1, 0, low), block(o, 2, 0, low)))
    for o in range(3):
        spread(o, 1)
        spread(o, 3)
    for o in range(3):
        relay(o, 0)
    take(ROW + 3, dh.at[1])
    dense[...] = (dot(dh[0], w_dd[0]) + dot(dh[1], w_dd[1])).astype(BF).astype(F32)
    for o in range(3):
        take(T2 + o, one(o))
        spread(o, 2)
    for o in range(3):
        relay(o, 1)
    for o in range(3):
        relay(o, 3)

    lane128 = lax.broadcasted_iota(jnp.int32, (16, 128), 1)
    rank16 = lax.broadcasted_iota(jnp.int32, (16, 128), 0).astype(F32) + 32.0
    lane256 = lax.broadcasted_iota(jnp.int32, (8, 256), 1)
    row256 = lax.broadcasted_iota(jnp.int32, (8, 256), 0)
    extra_rank = (row256 % 2).astype(F32) + 48.0
    extra_own = lane256 // 64 == row256 // 2
    first_half = lax.broadcasted_iota(jnp.int32, (8, 128), 1) < 64

    def eighth(i):
        return pl.ds(8 * (i % 2), 8)

    def pick(o, i):
        l0, w = LANES[o]
        a3 = ORDERS[o][2]
        code, weight = [], []
        for j in (0, 2):
            for into, at in ((code, 0), (weight, 128)):
                a = ag[o][i, j, ROWS:BLOCK, at : at + 128].astype(F32)
                b = ag[o][i, j + 1, ROWS:BLOCK, at : at + 128].astype(F32)
                into.append(jnp.where(first_half, a, b))
        code = jnp.concatenate(code, axis=1)
        weight = jnp.concatenate(weight, axis=1)
        for d in range(4):
            scale = power_of_two(jnp.full((8, 256), along(a3, d), jnp.int32))
            mine = (code >= 32.0 * scale) & (code < 64.0 * scale)
            ranks = jnp.sum(jnp.where(mine, code, F32(0.0)), axis=0, keepdims=True)
            weights = jnp.sum(jnp.where(mine, weight, F32(0.0)), axis=0, keepdims=True)
            unit = scale[0:1, 0:128]
            for j in range(4):
                lanes = slice(128 * (j // 2), 128 * (j // 2) + 128)
                hit = (ranks[:, lanes] == rank16 * unit) & ((lane128 // 64) == j % 2)
                at = slice(64 * d + 16 * j, 64 * d + 16 * j + 16)
                pick_m[o, at, lanes] = jnp.where(hit, F32(1.0), F32(0.0)).astype(BF)
                comb_m[4 * o + i, at, lanes] = jnp.where(hit, weights[:, lanes], F32(0.0)).astype(BF)
            hit = (ranks == extra_rank * scale[0:1]) & extra_own
            at = slice(256 + 8 * d, 256 + 8 * d + 8)
            pick_m[o, at] = jnp.where(hit, F32(1.0), F32(0.0)).astype(BF)
            comb_m[4 * o + i, at] = jnp.where(hit, weights, F32(0.0)).astype(BF)
        rows = dot(pick_m[o], ag[o][i, :, 0:ROWS, :].reshape(256, w)).astype(BF)
        for d in range(4):
            m = rows[64 * d : 64 * d + 64].reshape(4, 16, w)
            e = rows[256 + 8 * d : 256 + 8 * d + 8]
            if d == 0:
                xm[(0, *canonical(o, 0, i), ALL, pl.ds(l0, w))] = m
                xe[o][0, 0, i // 2, 8 * (i % 2) : 8 * (i % 2) + 8] = e
            else:
                cm[o][d - 1, i] = m
                ce[o][d - 1, i] = e
        far = next_dev[a3] if i % 2 == 0 else prev_dev[a3]
        go(FAR + 4 * o + i, one(o), far, (cm[o].at[1, i], fm[o].at[i]), (ce[o].at[1, i], fe[o].at[i]))

    def direct(o, i):
        l0, w = LANES[o]
        a3 = ORDERS[o][2]
        for source, d, dev in ((0, 3, next_dev[a3]), (2, 1, prev_dev[a3])):
            go(
                DIRECT + 4 * o + i, one(o), dev,
                (cm[o].at[source, i], xm.at[(0, *canonical(o, d, i), ALL, pl.ds(l0, w))]),
                (ce[o].at[source, i], xe[o].at[0, d, i // 2, eighth(i)]),
            )

    def pass_on(i):
        for o, (l0, w) in enumerate(LANES):
            a3 = ORDERS[o][2]
            take(FAR + 4 * o + i, one(o))
            go(
                PASSED + 4 * o + i, one(o), next_dev[a3] if i % 2 == 0 else prev_dev[a3],
                (fm[o].at[i], xm.at[(0, *canonical(o, 2, i), ALL, pl.ds(l0, w))]),
                (fe[o].at[i], xe[o].at[0, 2, i // 2, eighth(i)]),
            )

    def across(o, d, i):
        l0, w = LANES[o]
        at = (*canonical(o, d, i), ALL, pl.ds(l0, w))
        kind = 1 if d == 2 else 2 if i == 2 else 0
        go(CROSS + kind, fm[o].at[i], partner, (xm.at[(0, *at)], xm.at[(1, *at)]))

    def across_extra(o, d):
        go(EXTRA, xe[o].at[0, d], partner, (xe[o].at[0, d], xe[o].at[1, d]))

    def take_direct(i):
        for o in range(3):
            take(DIRECT + 4 * o + i, two(o))
            across(o, 3, i)
            across(o, 1, i)

    def take_passed(i):
        for o in range(3):
            take(PASSED + 4 * o + i, one(o))
            across(o, 2, i)

    def pick_unit(i):
        for o in range(3):
            pick(o, i)
        for o in range(3):
            direct(o, i)
        for o in range(3):
            across(o, 0, i)

    for o in range(3):
        relayed(o, 0)
    pick_unit(0)
    for o in range(3):
        relay(o, 2)
    for o in range(3):
        relayed(o, 1)
    pick_unit(1)
    for o in range(3):
        relayed(o, 3)
    pick_unit(3)
    for o in range(3):
        relayed(o, 2)
    for o in range(3):
        pick(o, 2)
    pass_on(0)
    for o in range(3):
        direct(o, 2)
        across(o, 0, 2)
    pass_on(1)
    pass_on(3)
    take_direct(0)
    take_direct(1)
    take_direct(3)
    pass_on(2)
    take_direct(2)
    for d in (0, 3, 1):
        for o in range(3):
            across_extra(o, d)
    take_passed(0)

    def gate_up(x_own, x_other, start, tag):
        size = x_own.shape[0]
        gate = dot(x_own, w_eg[0]) + dot(x_other, w_eg[1])
        up = dot(x_own, w_eu[0]) + dot(x_other, w_eu[1])
        hid[0, start : start + size] = (jax.nn.silu(gate) * up).astype(BF)
        span = pl.ds(start, size)
        go(HIDDEN + tag, hid.at[0, span], partner, (hid.at[0, span], hid.at[1, span]))

    def down(start, size, tag):
        take(HIDDEN + tag, hid.at[1, pl.ds(start, size)])
        at = slice(start, start + size)
        return (dot(hid[0, at], w_ed[0]) + dot(hid[1, at], w_ed[1])).astype(BF)

    def rows_of(c, groups):
        return jnp.concatenate([xm[(c, *g)].reshape(16 * n, HALF) for g, n in groups], axis=0)

    def put(y, groups):
        at = 0
        for g, n in groups:
            piece = y[at : at + 16 * n]
            ym[g] = piece.reshape(n, 16, HALF) if n > 1 else piece
            at += 16 * n

    early = [g for dz in NEAR for dy in NEAR for g in (((dz, dy, slice(0, 2)), 2), ((dz, dy, 3), 1))]
    mixed_rows = [g for dz in NEAR for g in (((dz, 2), 4), ((dz, 0, 2), 1), ((dz, 1, 2), 1), ((dz, 3, 2), 1))]
    landed(*expert_load)
    take(CROSS, xm.at[1, pl.ds(0, 3), pl.ds(0, 3)])
    gate_up(rows_of(0, early), rows_of(1, early), 0, 0)
    take_passed(1)
    take_passed(3)
    put(down(0, 432, 0), early)
    take_passed(2)
    for o in range(3):
        across_extra(o, 2)
    take(CROSS + 1, xm.at[1, 0])
    take(CROSS + 2, xm.at[1, pl.ds(0, 3), 0])
    gate_up(xm[0, 2].reshape(256, HALF), xm[1, 2].reshape(256, HALF), 432, 1)
    gate_up(rows_of(0, mixed_rows), rows_of(1, mixed_rows), 688, 2)
    take(EXTRA, xx.at[1])
    r128 = lax.broadcasted_iota(jnp.int32, (128, 128), 0)
    c128 = lax.broadcasted_iota(jnp.int32, (128, 128), 1)
    dz, dy, dx, bit = r128 // 32, (r128 // 8) % 4, (r128 // 2) % 4, r128 % 2
    turn = {
        0: (c128 == (dx * 16 + dz * 4 + dy) * 2 + bit).astype(BF),
        2: (c128 == (dy * 16 + dx * 4 + dz) * 2 + bit).astype(BF),
    }
    for c in range(2):
        for o, (l0, w) in enumerate(LANES):
            rows = xe[o][c].reshape(128, w)
            xx[c, :, l0 : l0 + w] = rows if o == 1 else dot(turn[o], rows).astype(BF)
    gate_up(xx[0], xx[1], 1024, 3)
    ym[2] = down(432, 256, 1).reshape(4, 4, 16, HALF)
    put(down(688, 336, 2), mixed_rows)
    yx[...] = down(1024, 128, 3)
    for o, (l0, w) in enumerate(LANES):
        rows = yx[:, l0 : l0 + w]
        rows = rows if o == 1 else dot_t(turn[o], rows).astype(BF)
        ye[o][...] = rows.reshape(4, 2, 16, w)

    def part(o, d, i):
        l0, w = LANES[o]
        return ym.at[(*canonical(o, d, i), ALL, pl.ds(l0, w))]

    def part_extra(o, d, i):
        return ye[o].at[d, i // 2, eighth(i)]

    def slot(o, d, i):
        return rm[o].at[i, pl.ds(4 * d, 4)]

    def slot_extra(o, d, i):
        return rm[o].at[i, 16 + d // 2, eighth(d)]

    def back_far(i):
        for o in range(3):
            a3 = ORDERS[o][2]
            go(
                BACK_FAR + 4 * o + i, one(o), next_dev[a3] if i % 2 == 0 else prev_dev[a3],
                (part(o, 2, i), gm[o].at[i]), (part_extra(o, 2, i), ge[o].at[i]),
            )

    def back_direct(i):
        for o in range(3):
            a3 = ORDERS[o][2]
            for d, dev in ((1, next_dev[a3]), (3, prev_dev[a3])):
                go(
                    BACK + 4 * o + i, one(o), dev,
                    (part(o, d, i), slot(o, 4 - d, i)), (part_extra(o, d, i), slot_extra(o, 4 - d, i)),
                )

    def pass_back(i):
        for o in range(3):
            a3 = ORDERS[o][2]
            take(BACK_FAR + 4 * o + i, one(o))
            go(
                BACK + 4 * o + i, one(o), next_dev[a3] if i % 2 == 0 else prev_dev[a3],
                (gm[o].at[i], slot(o, 2, i)), (ge[o].at[i], slot_extra(o, 2, i)),
            )

    def start_far(o, n, axis, src):
        sb[o][n, 0] = pt[o][src].astype(BF)
        half = sb[o].at[n, 0, pl.ds(0, 32)]
        go(SUM_A + 5 * o + n, half, prev_dev[axis], (half, rb[o].at[n, 0, pl.ds(0, 32)]))
        half = sb[o].at[n, 0, pl.ds(32, 32)]
        go(SUM_A + 5 * o + n, half, next_dev[axis], (half, rb[o].at[n, 0, pl.ds(32, 32)]))

    def start_near(o, n, axis, third, first):
        take(SUM_A + 5 * o + n, rb[o].at[n, 0])
        up32, low32 = slice(0, 32), slice(32, 64)
        sb[o][n, 1, 0:32] = (pt[o][(*third, up32)] + rb[o][n, 0, 0:32].astype(F32)).astype(BF)
        sb[o][n, 1, 32:64] = pt[o][(*third, low32)].astype(BF)
        sb[o][n, 2, 0:32] = pt[o][(*first, up32)].astype(BF)
        sb[o][n, 2, 32:64] = (pt[o][(*first, low32)] + rb[o][n, 0, 32:64].astype(F32)).astype(BF)
        go(SUM_B + 5 * o + n, sb[o].at[n, 1], prev_dev[axis], (sb[o].at[n, 1], rb[o].at[n, 1]))
        go(SUM_B + 5 * o + n, sb[o].at[n, 2], next_dev[axis], (sb[o].at[n, 2], rb[o].at[n, 2]))

    def finish(o, n, home):
        take(SUM_B + 5 * o + n, rb[o].at[n, pl.ds(1, 2)])
        pt[o][home] = pt[o][home] + rb[o][n, 1].astype(F32) + rb[o][n, 2].astype(F32)

    def combine(i):
        for o, (l0, w) in enumerate(LANES):
            take(BACK + 4 * o + i, three(o))
            sums = dot_t(comb_m[4 * o + i], rm[o][i].reshape(288, w))
            pt[o][i] = sums.reshape(4, ROWS, w)
            start_far(o, i, ORDERS[o][1], (i, 2))

    def near(i):
        for o in range(3):
            start_near(o, i, ORDERS[o][1], (i, 3), (i, 1))

    back_far(2)
    back_far(1)
    back_direct(2)
    back_far(3)
    back_direct(1)
    for o, (l0, w) in enumerate(LANES):
        for i in range(4):
            rm[o][i, 0:4] = ym[(*canonical(o, 0, i), ALL, slice(l0, l0 + w))]
            rm[o][i, 16, 0:8] = ye[o][0, i // 2, 8 * (i % 2) : 8 * (i % 2) + 8]
    pass_back(2)
    pass_back(1)
    back_direct(3)
    pass_back(3)
    back_far(0)
    back_direct(0)
    combine(2)
    combine(1)
    pass_back(0)
    combine(3)
    near(2)
    near(1)
    combine(0)
    near(3)
    for o in range(3):
        finish(o, 2, (2, 0))
        start_far(o, 4, ORDERS[o][0], (2, 0))
    near(0)
    for o in range(3):
        finish(o, 1, (1, 0))
    for o in range(3):
        finish(o, 3, (3, 0))
        start_near(o, 4, ORDERS[o][0], (3, 0), (1, 0))
    for o in range(3):
        finish(o, 0, (0, 0))
    for o, (l0, w) in enumerate(LANES):
        finish(o, 4, (0, 0))
        at = slice(l0, l0 + w)
        rest[:, at] = pt[o][0, 0] + scale_ref[:, at] * dense[:, at]
    for wait in sends[-SLOTS:]:
        wait.wait()


def layer(*args):
    vmem = pl.BlockSpec(memory_space=pltpu.VMEM)
    anyspace = pl.BlockSpec(memory_space=pl.ANY)
    widths = [w for _, w in LANES]
    per = lambda f, dt=BF: [pltpu.VMEM(f(w), dt) for w in widths]
    scratch = [
        pltpu.VMEM((ROWS, HALF), BF), pltpu.VMEM((6, ROWS), jnp.int32), pltpu.VMEM((6, ROWS), F32),
        pltpu.VMEM((1, 2048), F32), pltpu.VMEM((1, 2048), F32), pltpu.VMEM((4, HALF), F32),
        pltpu.VMEM((1, HALF), F32), pltpu.VMEM((1, HALF), F32),
        *[pltpu.VMEM((2, HALF, HALF), BF)] * 3,
        pltpu.VMEM((2, HALF, 256), BF), pltpu.VMEM((2, HALF, 256), BF), pltpu.VMEM((2, 256, HALF), BF),
        pltpu.VMEM((2, HALF, 256), BF), pltpu.VMEM((2, HALF, 256), BF), pltpu.VMEM((2, 256, HALF), BF),
        pltpu.VMEM((3, ROWS, HALF), BF), pltpu.VMEM((ROWS, HALF), F32),
        pltpu.VMEM((8, 128, 128), BF), pltpu.VMEM((8, 128, 128), BF),
        pltpu.VMEM((ROWS, HALF), BF), pltpu.VMEM((2, ROWS, HALF), BF), pltpu.VMEM((2, ROWS, HALF), BF),
        *per(lambda w: (4, 4, BLOCK, w)),
        *per(lambda w: (3, 4, 4, 16, w)),
        *per(lambda w: (3, 4, 8, w)),
        *per(lambda w: (4, 4, 16, w)),
        *per(lambda w: (4, 8, w)),
        pltpu.VMEM((2, 4, 4, 4, 16, HALF), BF),
        *per(lambda w: (2, 4, 2, 16, w)),
        pltpu.VMEM((2, 128, HALF), BF),
        pltpu.VMEM((2, 1152, 256), BF),
        pltpu.VMEM((4, 4, 4, 16, HALF), BF),
        pltpu.VMEM((128, HALF), BF),
        *per(lambda w: (4, 2, 16, w)),
        *per(lambda w: (4, 18, 16, w)),
        *per(lambda w: (4, 4, 16, w)),
        *per(lambda w: (4, 8, w)),
        *per(lambda w: (4, 4, ROWS, w), F32),
        *per(lambda w: (5, 3, ROWS, w)),
        *per(lambda w: (5, 3, ROWS, w)),
        pltpu.VMEM((3, 288, 256), BF), pltpu.VMEM((12, 288, 256), BF),
        pltpu.VMEM((2, ROWS, 256), BF), pltpu.VMEM((ROWS, HALF), F32),
        pltpu.SemaphoreType.DMA((SLOTS,)), pltpu.SemaphoreType.DMA((102,)), pltpu.SemaphoreType.DMA((22,)),
    ]
    wide = pltpu.VMEM((ROWS, HALF), F32)
    short = pltpu.VMEM((ROWS, HALF), BF)
    return pl.pallas_call(
        layer_kernel,
        out_shape=(wide, short, short, wide, wide),
        in_specs=[anyspace] * 21,
        out_specs=(vmem,) * 5,
        scratch_shapes=scratch,
        compiler_params=pltpu.CompilerParams(
            collective_id=0, has_side_effects=True, vmem_limit_bytes=56 * 1024 * 1024
        ),
        name="layer",
    )(*args)


def outputs_kernel(conv_hbm, rest, resid, branch, kept, driven, result, state, conv, r_buf, s_buf, c_buf, sems):
    old = pltpu.make_async_copy(conv_hbm.at[pl.ds(1, 2)], c_buf, sems.at[0])
    old.start()
    last = pltpu.make_async_copy(branch, conv.at[2], sems.at[1])
    last.start()
    s_buf[...] = kept[...] + driven[...]
    state_copy = pltpu.make_async_copy(s_buf, state, sems.at[2])
    state_copy.start()
    r_buf[...] = (resid[...].astype(F32) + rest[...]).astype(BF)
    result_copy = pltpu.make_async_copy(r_buf, result, sems.at[3])
    result_copy.start()
    old.wait()
    moved = pltpu.make_async_copy(c_buf, conv.at[pl.ds(0, 2)], sems.at[4])
    moved.start()
    for copy in (last, state_copy, result_copy, moved):
        copy.wait()


def outputs(*args):
    vmem = pl.BlockSpec(memory_space=pltpu.VMEM)
    anyspace = pl.BlockSpec(memory_space=pl.ANY)
    return pl.pallas_call(
        outputs_kernel,
        out_shape=(
            jax.ShapeDtypeStruct((ROWS, HALF), BF),
            jax.ShapeDtypeStruct((ROWS, HALF), F32),
            jax.ShapeDtypeStruct((3, ROWS, HALF), BF),
        ),
        in_specs=[anyspace] + [vmem] * 5,
        out_specs=(anyspace,) * 3,
        scratch_shapes=[
            pltpu.VMEM((ROWS, HALF), BF), pltpu.VMEM((ROWS, HALF), F32), pltpu.VMEM((2, ROWS, HALF), BF),
            pltpu.SemaphoreType.DMA((5,)),
        ],
        compiler_params=pltpu.CompilerParams(vmem_limit_bytes=4 * 1024 * 1024),
        name="outputs",
    )(*args)


def per_device(
    stream, conv_state, recur_state, mix_gain, branch_weight, gate_weight, conv_taps, recur_map, input_map,
    decay_logit, out_weight, moe_gain, route_ids, route_weights, expert_gate, expert_up, expert_down,
    dense_gate, dense_up, dense_down, dense_scale,
):
    conv_turned = jnp.transpose(conv_state, (1, 0, 2))
    parts = layer(
        stream, route_ids.T, route_weights.T, mix_gain.reshape(1, -1), moe_gain.reshape(1, -1), conv_taps,
        decay_logit.reshape(1, -1), dense_scale.reshape(1, -1), conv_turned, recur_state,
        recur_map, input_map, branch_weight, gate_weight, out_weight,
        expert_gate, expert_up, expert_down, dense_gate, dense_up, dense_down,
    )
    result, new_state, new_conv = outputs(conv_turned, *parts)
    return (result, new_state, jnp.transpose(new_conv, (1, 0, 2)))


def solution(mesh):
    in_specs = (
        P("ep", "tp"), P("ep", None, "tp"), P("ep", "tp"), P(), P(None, "tp"), P(None, "tp"), P(None, "tp"),
        P("tp", None, None), P("tp", None, None), P("tp"), P(None, "tp"), P(), P("ep", None), P("ep", None),
        P("ep", None, "tp"), P("ep", None, "tp"), P("ep", None, "tp"), P(None, "tp"), P(None, "tp"),
        P(None, "tp"), P("tp"),
    )
    out_specs = (P("ep", "tp"), P("ep", "tp"), P("ep", None, "tp"))
    return jax.shard_map(per_device, mesh=mesh, in_specs=in_specs, out_specs=out_specs, check_vma=False)
```

time: 85.4 us -> 71.7 us (0.84)
  Pallas kernels: 84.4 us -> 70.9 us
    pallas_call x1, Pallas kernels: 81.3 us -> 70 us  [layer(): pl.pallas_call(layer_kernel, out_shape=(wide, short, short, wide, wide),...]
    pallas_call x1, Pallas kernels: 3.06 us -> 0.94 us  [outputs(): pl.pallas_call(outputs_kernel, out_shape=(jax.ShapeDtypeStruct((ROWS, HAL...]
where the time goes in v3:
time: 71.7 us; the launch traced here: 71.6 us
  Pallas kernels  70.9 us (99%)
    pallas_call x1, Pallas kernels, layer(): pl.pallas_call(layer_kernel, out_shape=(wide, short, short, wide, wide),...  70 us

profile of v3, /device:TPU:0, one launch (start us, length us, event | category | flops | bytes accessed | tf_op | source)
XLA Modules:
  0.0 71.6 jit_solution(6698905153717876630)
XLA Ops:
  0.6 0.0 copy-start
  0.6 70.0 %layer.1 = (f32[64,1024]{1,0:T(8,128)S(1)}, bf16[64,1024]{1,0:T(8,128)(2,1)S(1)}, bf16[64,1024]{1,0:T(8,128)(2,1)S(1)}, f32[64,1024]{1,0:T(8,128)S(1)}, f32[64,1024]{1,0:T(8,128)S(1)}) custom-call(bf16[64,1024]{1,0:T(8,128)(2,1)} %stream_hbm.1, s32[6,64]{1,0:T(8,128)} %bitcast.12, f32[6,64]{1,0:T(8,128)} %bitcast.13, f32[1,2048]{1,0:T(1,128)} %bitcast.10, ...), custom_call_target="tpu_custom_call" | custom-call | tf_op jit(solution)/shard_map/layer/pallas_call | solution.py:632
  70.6 0.0 copy-done
  70.7 0.9 %outputs.1 = (bf16[64,1024]{1,0:T(8,128)(2,1)}, f32[64,1024]{1,0:T(8,128)}, bf16[3,64,1024]{2,1,0:T(8,128)(2,1)}) custom-call(bf16[3,64,1024]{2,1,0:T(8,128)(2,1)S(1)} %bitcast.9, f32[64,1024]{1,0:T(8,128)S(1)} %get-tuple-element.11.rest, bf16[64,1024]{1,0:T(8,128)(2,1)S(1)} %get-tuple-element.12.resid, bf16[64,1024]{1,0:T(8,128)(2,1)S(1)} %get-tuple-element.13.branch, ...), custom_call_target="tpu_custom_call" | custom-call | tf_op jit(solution)/shard_map/outputs/pallas_call | solution.py:666
Async XLA Ops:
  0.6 70.0 %copy-start = (bf16[64,3,1024]{2,0,1:T(8,128)(2,1)S(1)}, bf16[64,3,1024]{2,0,1:T(8,128)(2,1)}, u32[]{:S(2)}) copy-start(bf16[64,3,1024]{2,0,1:T(8,128)(2,1)} %param.22) | copy-start | bytes 1179652
